TPU v7x, 32 devices: a whole 2x2x4 slice. The times are simulated.
32 devices in a mesh: sp: 16 (over z, y, x), tp: 2 (over core).
Axes of the slice: x: 2, y: 2, z: 4, core: 2. Of those that a mesh axis runs over, the one named last changes fastest.
Arguments:
- latent: bfloat16 [4096, 256], P('sp'), may hold values from -6 to 6
- rotary_key: bfloat16 [4096, 64], P('sp'), may hold values from -7 to 7
- doc_ids: int32 [4096], P('sp'), may hold values from 0 to 7, never falling along the last dimension, each value on 1 to 1024 neighbouring positions
- queries_content: bfloat16 [4096, 1024], P('sp', 'tp'), may hold values from -6 to 6
- queries_rotary: bfloat16 [4096, 512], P('sp', 'tp'), may hold values from -400 to 400
- w_key_up: bfloat16 [256, 1024], replicated, may hold values from -0.375 to 0.375
- w_value_up: bfloat16 [256, 1024], replicated, may hold values from -0.375 to 0.375
- w_out: bfloat16 [1024, 2048], P('tp'), may hold values from -1.5 to 1.5
- residual: bfloat16 [4096, 2048], P(('sp', 'tp')), may hold values from -4 to 4
- norm_gain: float32 [2048], replicated, may hold values from 0.1 to 1.9
- routes: int32 [4096, 2], P(('sp', 'tp')), may hold values from 0 to 15, all different within a row; in each aligned block of 128 rows (0 to 127, 128 to 255, ...) at most 32 rows name the same one
- route_weights: float32 [4096, 2], P(('sp', 'tp')), may hold values from 0.1 to 1
- w_gate: bfloat16 [16, 2048, 3584], P('sp', None, 'tp'), may hold values from -0.125 to 0.125
- w_up: bfloat16 [16, 2048, 3584], P('sp', None, 'tp'), may hold values from -0.125 to 0.125
- w_down: bfloat16 [16, 3584, 2048], P('sp', 'tp'), may hold values from -0.09375 to 0.09375
- out_gain: float32 [2048], replicated, may hold values from 0.1 to 1.9
Outputs:
- mixed: bfloat16 [4096, 2048], P(('sp', 'tp'))
Inputs may be any that keep to these rules, and one draw needn't show every extreme that they name: `doc_ids`: document numbers never fall along positions; each document holds 1 to 1024 positions, and one holds exactly 1024. `routes`: each row names 2 different experts; among the rows of one device (aligned blocks of 128 rows) no expert is named more than 32 times, and in some blocks one expert is named exactly 32 times.
All inputs are finite; a program needn't handle non-finite values.
Results may differ from a plain program's by a relative error of at most 0.014.
Values may be sent and summed in bfloat16 or wider, within the bound.
No kernel may reach another device: no remote copies, remote signals or barrier semaphores. Data moves between devices by JAX's collectives and lax.ppermute only.
A program may use at most 128 MiB of HBM per device.

v0:
```python
import jax
import jax.numpy as jnp
from jax import lax
from jax.sharding import PartitionSpec as P

HEADS = 8
DK = 128
DR = 64
DV = 128
TOPK = 2
REACH = 4


ROPE_THETA = 500000.0
RESIDUAL_SCALE = 2.0**0.5
NORM_EPSILON = 1e-05


def shifted(value, axis, steps):
    count = lax.axis_size(axis)
    leading, last = (max(0, -steps), min(count, count - steps))
    return lax.ppermute(value, axis, [(source, source + steps) for source in range(leading, last)])


def rotate(values, positions):
    half_width = values.shape[-1] // 2
    frequency = ROPE_THETA ** (-2.0 * jnp.arange(half_width, dtype=jnp.float32) / values.shape[-1])
    angles = positions.astype(jnp.float32)[:, None] * frequency[None, :]
    table_shape = (values.shape[0],) + (1,) * (values.ndim - 2) + (half_width,)
    cosine = jnp.cos(angles).reshape(table_shape)
    sine_part = jnp.sin(angles).reshape(table_shape)
    widened = values.astype(jnp.float32)
    first_half = widened[..., :half_width]
    second = widened[..., half_width:]
    return jnp.concatenate(
        [first_half * cosine - second * sine_part, second * cosine + first_half * sine_part], -1
    )


def layer_norm(values, gain_vec):
    centre = jnp.mean(values, -1, keepdims=True)
    spread = jnp.mean(jnp.square(values - centre), -1, keepdims=True)
    return (values - centre) * lax.rsqrt(spread + NORM_EPSILON) * gain_vec


def per_device(
    latent,
    rotary_key,
    doc_ids,
    queries_content,
    queries_rotary,
    w_key_up,
    w_value_up,
    w_out,
    residual,
    norm_gain,
    routes,
    route_weights,
    w_gate,
    w_up,
    w_down,
    out_gain,
):
    tok_dev = latent.shape[0]
    core_count = lax.axis_size("tp")
    chip_count = lax.axis_size("sp")
    heads_here = HEADS // core_count
    head_index = lax.axis_index("tp")
    sp_index = lax.axis_index("sp")
    key_cols = lax.dynamic_slice_in_dim(w_key_up, head_index * heads_here * DK, heads_here * DK, 1)
    value_cols = lax.dynamic_slice_in_dim(
        w_value_up, head_index * heads_here * DV, heads_here * DV, 1
    )
    own_position = sp_index * tok_dev + jnp.arange(tok_dev, dtype=jnp.int32)
    query_turned = rotate(queries_rotary.reshape(tok_dev, heads_here, DR), own_position).astype(
        jnp.bfloat16
    )
    query_block = queries_content.reshape(tok_dev, heads_here, DK)
    pieces = [(latent, rotary_key, doc_ids)]
    for distance in range(1, REACH + 1):
        pieces.append(shifted((latent, rotary_key, doc_ids), "sp", distance))
    ordered = pieces[::-1]
    key_latent = jnp.concatenate([piece[0] for piece in ordered], 0)
    key_rope = jnp.concatenate([piece[1] for piece in ordered], 0)
    key_doc = jnp.concatenate([piece[2] for piece in ordered], 0)
    key_count = key_latent.shape[0]
    key_position = (sp_index - REACH) * tok_dev + jnp.arange(key_count, dtype=jnp.int32)
    key_content = jnp.dot(key_latent, key_cols, preferred_element_type=jnp.float32).astype(
        jnp.bfloat16
    )
    key_content = key_content.reshape(key_count, heads_here, DK)
    values = jnp.dot(key_latent, value_cols, preferred_element_type=jnp.float32).astype(
        jnp.bfloat16
    )
    values = values.reshape(key_count, heads_here, DV)
    key_turned = rotate(key_rope, key_position).astype(jnp.bfloat16)
    score_scale = (DK + DR) ** (-0.5)
    scores = jnp.einsum(
        "phd,qhd->hpq", query_block, key_content, preferred_element_type=jnp.float32
    )
    scores = scores + jnp.einsum(
        "phd,qd->hpq", query_turned, key_turned, preferred_element_type=jnp.float32
    )
    scores = scores * score_scale
    allowed = (key_position[None, :] <= own_position[:, None]) & (key_position[None, :] >= 0)
    allowed = allowed & (key_doc[None, :] == doc_ids[:, None])
    scores = jnp.where(allowed[None], scores, -jnp.inf)
    row_peak = jnp.max(scores, -1, keepdims=True)
    lifted = jnp.exp(scores - row_peak)
    probability = (lifted / jnp.sum(lifted, -1, keepdims=True)).astype(jnp.bfloat16)
    attended = jnp.einsum("hpq,qhd->phd", probability, values, preferred_element_type=jnp.float32)
    attended = attended.astype(jnp.bfloat16).reshape(tok_dev, heads_here * DV)
    partial_value = jnp.dot(attended, w_out, preferred_element_type=jnp.float32)
    projected = lax.psum_scatter(
        partial_value.astype(jnp.bfloat16).astype(jnp.float32).astype(jnp.bfloat16),
        "tp",
        scatter_dimension=0,
        tiled=True,
    ).astype(jnp.float32)
    normed = layer_norm(
        RESIDUAL_SCALE * residual.astype(jnp.float32) + projected, norm_gain
    ).astype(jnp.bfloat16)
    row_count = normed.shape[0]
    model_width = normed.shape[1]
    capacity = max(2, 2 * row_count * TOPK // chip_count)
    flat_route = routes.reshape(-1)
    member = (flat_route[:, None] == jnp.arange(chip_count, dtype=jnp.int32)[None, :]).astype(
        jnp.int32
    )
    slot_rank = jnp.sum((jnp.cumsum(member, 0) - member) * member, 1)
    slot_index = flat_route * capacity + slot_rank
    placing = (
        slot_index[None, :] == jnp.arange(chip_count * capacity, dtype=jnp.int32)[:, None]
    ).astype(jnp.int32)
    placing = jnp.sum(placing.reshape(chip_count * capacity, row_count, TOPK), -1).astype(
        jnp.bfloat16
    )
    outbound = jnp.dot(placing, normed, preferred_element_type=jnp.float32).astype(jnp.bfloat16)
    outbound = outbound.reshape(chip_count, capacity, model_width)
    landed = lax.all_to_all(outbound, "sp", split_axis=0, concat_axis=0, tiled=True)
    arrived = lax.all_gather(landed[:, None], "tp", axis=1, tiled=True)
    flat_rows = arrived.reshape(-1, model_width)
    gate_pre = jnp.dot(flat_rows, w_gate[0], preferred_element_type=jnp.float32)
    upward = jnp.dot(flat_rows, w_up[0], preferred_element_type=jnp.float32)
    hidden = (jax.nn.silu(gate_pre) * upward).astype(jnp.bfloat16)
    partial_value = jnp.dot(hidden, w_down[0], preferred_element_type=jnp.float32)
    partial_value = (
        partial_value.astype(jnp.bfloat16)
        .astype(jnp.float32)
        .reshape(chip_count, core_count, capacity, model_width)
    )
    reduced = lax.psum_scatter(
        partial_value.astype(jnp.bfloat16), "tp", scatter_dimension=1, tiled=True
    )
    returned = lax.all_to_all(
        reduced.reshape(chip_count, capacity, model_width),
        "sp",
        split_axis=0,
        concat_axis=0,
        tiled=True,
    )
    returned = returned.reshape(chip_count * capacity, model_width)
    picked = (
        jnp.take(returned, slot_index, axis=0)
        .reshape(row_count, TOPK, model_width)
        .astype(jnp.float32)
    )
    routed_sum = jnp.sum(picked * route_weights[:, :, None], 1)
    combined = RESIDUAL_SCALE * normed.astype(jnp.float32) + routed_sum
    return layer_norm(combined, out_gain).astype(jnp.bfloat16)


def solution(mesh):
    return jax.shard_map(
        per_device,
        mesh=mesh,
        in_specs=(
            P("sp", None),
            P("sp", None),
            P("sp"),
            P("sp", "tp"),
            P("sp", "tp"),
            P(),
            P(),
            P("tp", None),
            P(("sp", "tp"), None),
            P(),
            P(("sp", "tp"), None),
            P(("sp", "tp"), None),
            P("sp", None, "tp"),
            P("sp", None, "tp"),
            P("sp", "tp", None),
            P(),
        ),
        out_specs=P(("sp", "tp"), None),
        check_vma=False,
    )
```

profile of v0, /device:TPU:16, one launch (start us, length us, event | category | flops | bytes accessed | tf_op | source)
XLA Modules:
  0.0 322.2 jit_solution(12835083971645171798)
XLA Ops:
  6.5 3.6 %collective-permute-start = (bf16[256,256]{1,0:T(8,128)(2,1)}, bf16[256,256]{1,0:T(8,128)(2,1)S(1)}, u32[]{:S(2)}, u32[]{:S(2)}) collective-permute-start(bf16[256,256]{1,0:T(8,128)(2,1)} %param.16), channel_id=1, source_target_pairs={{0,8},{2,10},{4,12},{6,14},{8,16},{10,18},{12,20},{14,22},{16,24},... | collective-permute-start | bytes 393224 | tf_op jit(solution)/shard_map/ppermute | solution.py:22
  10.2 4.4 %collective-permute-start.1 = (bf16[256,256]{1,0:T(8,128)(2,1)}, bf16[256,256]{1,0:T(8,128)(2,1)S(1)}, u32[]{:S(2)}, u32[]{:S(2)}) collective-permute-start(bf16[256,256]{1,0:T(8,128)(2,1)} %param.16), channel_id=1, source_target_pairs={{0,6},{2,8},{4,10},{6,12},{8,14},{10,16},{12,18},{14,20},{16,22},{... | collective-permute-start | bytes 393224 | tf_op jit(solution)/shard_map/ppermute | solution.py:22
  14.5 1.9 collective-permute-start.2
  16.5 2.5 collective-permute-start.3
  18.9 1.9 collective-permute-start.4
  22.2 2.4 collective-permute-done.4
  24.6 3.7 %collective-permute-start.5 = (s32[256]{0:T(256)}, s32[256]{0:T(256)S(1)}, u32[]{:S(2)}, u32[]{:S(2)}) collective-permute-start(s32[256]{0:T(256)} %param.18), channel_id=1, source_target_pairs={{0,6},{2,8},{4,10},{6,12},{8,14},{10,16},{12,18},{14,20},{16,22},{... | collective-permute-start | bytes 3080 | tf_op jit(solution)/shard_map/ppermute | solution.py:22
  28.3 3.7 %collective-permute-done.5 = s32[256]{0:T(256)S(1)} collective-permute-done((s32[256]{0:T(256)}, s32[256]{0:T(256)S(1)}, u32[]{:S(2)}, u32[]{:S(2)}) %collective-permute-start.5) | collective-permute-done | bytes 1056 | tf_op jit(solution)/shard_map/ppermute | solution.py:22
  32.1 1.9 collective-permute-start.6
  34.0 4.6 %collective-permute-done.6 = s32[256]{0:T(256)S(1)} collective-permute-done((s32[256]{0:T(256)}, s32[256]{0:T(256)S(1)}, u32[]{:S(2)}, u32[]{:S(2)}) %collective-permute-start.6) | collective-permute-done | bytes 1056 | tf_op jit(solution)/shard_map/ppermute | solution.py:22
  38.7 4.3 %collective-permute-start.7 = (s32[256]{0:T(256)}, s32[256]{0:T(256)S(1)}, u32[]{:S(2)}, u32[]{:S(2)}) collective-permute-start(s32[256]{0:T(256)} %param.18), channel_id=1, source_target_pairs={{0,2},{2,4},{4,6},{6,8},{8,10},{10,12},{12,14},{14,16},{16,18},{18... | collective-permute-start | bytes 3080 | tf_op jit(solution)/shard_map/ppermute | solution.py:22
  42.9 3.2 collective-permute-done.7
  54.1 5.0 %collective-permute-done.9 = bf16[256,64]{0,1:T(8,128)(2,1)S(1)} collective-permute-done((bf16[256,64]{0,1:T(8,128)(2,1)}, bf16[256,64]{0,1:T(8,128)(2,1)S(1)}, u32[]{:S(2)}, u32[]{:S(2)}) %collective-permute-start.9) | collective-permute-done | bytes 32800 | tf_op jit(solution)/shard_map/ppermute | solution.py:22
  59.0 2.4 collective-permute-start.10
  61.4 4.5 %collective-permute-done.10 = bf16[256,64]{0,1:T(8,128)(2,1)S(1)} collective-permute-done((bf16[256,64]{0,1:T(8,128)(2,1)}, bf16[256,64]{0,1:T(8,128)(2,1)S(1)}, u32[]{:S(2)}, u32[]{:S(2)}) %collective-permute-start.10) | collective-permute-done | bytes 32800 | tf_op jit(solution)/shard_map/ppermute | solution.py:22
  65.9 3.4 %collective-permute-start.11 = (bf16[256,64]{0,1:T(8,128)(2,1)}, bf16[256,64]{0,1:T(8,128)(2,1)S(1)}, u32[]{:S(2)}, u32[]{:S(2)}) collective-permute-start(bf16[256,64]{0,1:T(8,128)(2,1)} %param.17), channel_id=1, source_target_pairs={{0,2},{2,4},{4,6},{6,8},{8,10},{10,12},{12,14},{14,16},{16,18},{18... | collective-permute-start | bytes 98312 | tf_op jit(solution)/shard_map/ppermute | solution.py:22
  69.3 4.4 %collective-permute-done.11 = bf16[256,64]{0,1:T(8,128)(2,1)S(1)} collective-permute-done((bf16[256,64]{0,1:T(8,128)(2,1)}, bf16[256,64]{0,1:T(8,128)(2,1)S(1)}, u32[]{:S(2)}, u32[]{:S(2)}) %collective-permute-start.11) | collective-permute-done | bytes 32800 | tf_op jit(solution)/shard_map/ppermute | solution.py:22
  79.7 2.3 copy-done.2
  83.7 6.2 %fusion.16 = bf16[4,128,256]{2,1,0:T(8,128)(2,1)} fusion(bf16[1280,4,128]{0,2,1:T(8,128)(2,1)S(1)} %bitcast.94, f32[4,256]{1,0:T(4,128)S(1)} %exponential_reduce_fusion, f32[4,256,1280]{1,2,0:T(8,128)} %copy-done.2), kind=kOutput, calls=%fused_computation.25 | convolution fusion | flops 339609856 | bytes 6819840 | tf_op jit(solution)/shard_map/hpq,qhd->phd/dot_general | solution.py:111
  89.9 2.7 convolution_convert_fusion.3
  94.3 5.4 %reduce-scatter.5.cloned.1.call-done = bf16[128,2048]{1,0:T(8,128)(2,1)} async-done(((bf16[256,2048]{1,0:T(8,128)(2,1)}), bf16[128,2048]{1,0:T(8,128)(2,1)}) %reduce-scatter.5.cloned.1.call-update) | async-done | bytes 524304 | tf_op jit(solution)/shard_map/reduce_scatter | solution.py:114
  104.4 54.0 %all_to_all.10 = bf16[16,32,2048]{2,1,0:T(8,128)(2,1)} all-to-all(bf16[16,32,2048]{2,1,0:T(8,128)(2,1)S(1)} %bitcast.91), channel_id=1, replica_groups=mesh['sp'=16,'tp'=2] {'sp'}, dimensions={0} | all-to-all | bytes 4194304 | tf_op jit(solution)/shard_map/all_to_all | solution.py:140
  158.6 13.8 %all-gather.3.cloned.1.call-done = bf16[16,64,2048]{2,1,0:T(8,128)(2,1)} async-done(((bf16[16,32,2048]{2,1,0:T(8,128)(2,1)}), bf16[16,64,2048]{2,1,0:T(8,128)(2,1)}) %all-gather.3.cloned.1.call-update) | async-done | bytes 4194320 | tf_op jit(solution)/shard_map/all_gather | solution.py:141
  172.4 13.5 %fusion.5 = f32[1024,1792]{1,0:T(8,128)} fusion(bf16[1024,2048]{1,0:T(8,128)(2,1)} %bitcast.99, bf16[1,2048,1792]{2,1,0:T(8,128)(2,1)} %param.28), kind=kOutput, calls=%fused_computation.6 | convolution fusion | flops 7516192768 | bytes 18874368 | tf_op jit(solution)/shard_map/dot_general | solution.py:143
  185.9 25.8 %fusion.12 = bf16[1024,2048]{1,0:T(8,128)(2,1)} fusion(bf16[1,1792,2048]{2,1,0:T(8,128)(2,1)} %param.30, f32[1024,1792]{1,0:T(8,128)} %fusion.5, bf16[1024,2048]{1,0:T(8,128)(2,1)} %bitcast.100, bf16[1,2048,1792]{2,1,0:T(8,128)(2,1)} %param.29), kind=kOutput, calls=%fused_computation.15 | convolution fusion | flops 15045492736 | bytes 30408704 | tf_op jit(solution)/shard_map/dot_general | solution.py:146
  212.4 28.8 %all-reduce.3.cloned.1.call-done = bf16[16,2,32,2048]{3,2,1,0:T(8,128)(2,1)} async-done(((bf16[16,2,32,2048]{3,2,1,0:T(8,128)(2,1)}), bf16[16,2,32,2048]{3,2,1,0:T(8,128)(2,1)}) %all-reduce.3.cloned.1.call-update) | async-done | bytes 4194320
  241.2 3.8 %dynamic-slice_bitcast_fusion = bf16[16,32,2048]{2,1,0:T(8,128)(2,1)} fusion(bf16[16,2,32,2048]{3,2,1,0:T(8,128)(2,1)} %all-reduce.3.cloned.1.call-done, u32[]{:T(128)} %bitcast.26), kind=kLoop, calls=%fused_computation.21 | loop fusion | bytes 4194308 | tf_op jit(solution)/shard_map/reshape | solution.py:156
  245.0 7.0 %all-to-all-start.1 = ((bf16[16,32,2048]{2,1,0:T(8,128)(2,1)}), bf16[16,32,2048]{2,1,0:T(8,128)(2,1)}, u32[]{:S(2)}, u32[]{:S(2)}) async-start(bf16[16,32,2048]{2,1,0:T(8,128)(2,1)} %dynamic-slice_bitcast_fusion), calls=%async_computation.2 | async-start | bytes 4194304 | tf_op jit(solution)/shard_map/all_to_all | solution.py:155
  252.5 48.1 %all-to-all-done.1 = bf16[16,32,2048]{2,1,0:T(8,128)(2,1)} async-done(((bf16[16,32,2048]{2,1,0:T(8,128)(2,1)}), bf16[16,32,2048]{2,1,0:T(8,128)(2,1)}, u32[]{:S(2)}, u32[]{:S(2)}) %all-to-all-start.1) | async-done | bytes 2097184 | tf_op jit(solution)/shard_map/all_to_all | solution.py:155
  300.6 5.4 %gather_fusion = bf16[256,2048]{1,0:T(8,128)(2,1)} fusion(bf16[512,2048]{1,0:T(8,128)(2,1)} %bitcast.16, s32[1024]{0:T(1024)S(1)} %pad_clamp_fusion), kind=kCustom, calls=%fused_computation | custom fusion | bytes 2098176 | tf_op jit(solution)/shard_map/jit(_take)/gather | solution.py:164
  305.9 2.6 gather.7
  308.5 5.5 %multiply_reduce_fusion = f32[128,2048]{1,0:T(8,128)S(1)} fusion(bf16[128,2,2048]{2,1,0:T(2,128)(2,1)} %gather.7, pred[128,2]{1,0:T(8,128)(4,1)S(1)} %copy.60, f32[128,2]{1,0:T(8,128)S(1)} %copy.62), kind=kLoop, calls=%fused_computation.22 | loop fusion | flops 1835008 | bytes 2098432 | tf_op jit(solution)/shard_map/reduce_sum | solution.py:168
  (99 shorter events, 26.1 us)
Async XLA Ops:
  6.5 83.3 %copy-start = (bf16[512,2048]{1,0:T(8,128)(2,1)S(1)}, bf16[512,2048]{1,0:T(8,128)(2,1)}, u32[]{:S(2)}) copy-start(bf16[512,2048]{1,0:T(8,128)(2,1)} %param.23) | copy-start | bytes 6291460
  6.5 71.2 %copy-start.4 = (bf16[256,512]{1,0:T(8,128)(2,1)S(1)}, bf16[256,512]{1,0:T(8,128)(2,1)}, u32[]{:S(2)}) copy-start(bf16[256,512]{1,0:T(8,128)(2,1)} %param.19) | copy-start | bytes 786436
  6.5 93.1 %reduce-scatter.5.cloned.1.call-start = ((), (), s32[]{:S(2)}) async-start(), calls=%async_computation.3 | async-start | bytes 1572864 | tf_op jit(solution)/shard_map/reduce_scatter | solution.py:114
  6.5 68.7 %collective-permute-start = (bf16[256,256]{1,0:T(8,128)(2,1)}, bf16[256,256]{1,0:T(8,128)(2,1)S(1)}, u32[]{:S(2)}, u32[]{:S(2)}) collective-permute-start(bf16[256,256]{1,0:T(8,128)(2,1)} %param.16), channel_id=1, source_target_pairs={{0,8},{2,10},{4,12},{6,14},{8,16},{10,18},{12,20},{14,22},{16,24},... | collective-permute-start | bytes 393224 | tf_op jit(solution)/shard_map/ppermute | solution.py:22
  10.2 65.1 %collective-permute-start.1 = (bf16[256,256]{1,0:T(8,128)(2,1)}, bf16[256,256]{1,0:T(8,128)(2,1)S(1)}, u32[]{:S(2)}, u32[]{:S(2)}) collective-permute-start(bf16[256,256]{1,0:T(8,128)(2,1)} %param.16), channel_id=1, source_target_pairs={{0,6},{2,8},{4,10},{6,12},{8,14},{10,16},{12,18},{14,20},{16,22},{... | collective-permute-start | bytes 393224 | tf_op jit(solution)/shard_map/ppermute | solution.py:22
  14.5 60.8 %collective-permute-start.2 = (bf16[256,256]{1,0:T(8,128)(2,1)}, bf16[256,256]{1,0:T(8,128)(2,1)S(1)}, u32[]{:S(2)}, u32[]{:S(2)}) collective-permute-start(bf16[256,256]{1,0:T(8,128)(2,1)} %param.16), channel_id=1, source_target_pairs={{0,4},{2,6},{4,8},{6,10},{8,12},{10,14},{12,16},{14,18},{16,20},{1... | collective-permute-start | bytes 393224 | tf_op jit(solution)/shard_map/ppermute | solution.py:22
  16.5 58.9 %collective-permute-start.3 = (bf16[256,256]{1,0:T(8,128)(2,1)}, bf16[256,256]{1,0:T(8,128)(2,1)S(1)}, u32[]{:S(2)}, u32[]{:S(2)}) collective-permute-start(bf16[256,256]{1,0:T(8,128)(2,1)} %param.16), channel_id=1, source_target_pairs={{0,2},{2,4},{4,6},{6,8},{8,10},{10,12},{12,14},{14,16},{16,18},{18... | collective-permute-start | bytes 393224 | tf_op jit(solution)/shard_map/ppermute | solution.py:22
  18.9 5.7 %collective-permute-start.4 = (s32[256]{0:T(256)}, s32[256]{0:T(256)S(1)}, u32[]{:S(2)}, u32[]{:S(2)}) collective-permute-start(s32[256]{0:T(256)} %param.18), channel_id=1, source_target_pairs={{0,8},{2,10},{4,12},{6,14},{8,16},{10,18},{12,20},{14,22},{16,24},... | collective-permute-start | bytes 3080 | tf_op jit(solution)/shard_map/ppermute | solution.py:22
  24.6 7.5 %collective-permute-start.5 = (s32[256]{0:T(256)}, s32[256]{0:T(256)S(1)}, u32[]{:S(2)}, u32[]{:S(2)}) collective-permute-start(s32[256]{0:T(256)} %param.18), channel_id=1, source_target_pairs={{0,6},{2,8},{4,10},{6,12},{8,14},{10,16},{12,18},{14,20},{16,22},{... | collective-permute-start | bytes 3080 | tf_op jit(solution)/shard_map/ppermute | solution.py:22
  32.1 6.6 %collective-permute-start.6 = (s32[256]{0:T(256)}, s32[256]{0:T(256)S(1)}, u32[]{:S(2)}, u32[]{:S(2)}) collective-permute-start(s32[256]{0:T(256)} %param.18), channel_id=1, source_target_pairs={{0,4},{2,6},{4,8},{6,10},{8,12},{10,14},{12,16},{14,18},{16,20},{1... | collective-permute-start | bytes 3080 | tf_op jit(solution)/shard_map/ppermute | solution.py:22
  38.7 7.5 %collective-permute-start.7 = (s32[256]{0:T(256)}, s32[256]{0:T(256)S(1)}, u32[]{:S(2)}, u32[]{:S(2)}) collective-permute-start(s32[256]{0:T(256)} %param.18), channel_id=1, source_target_pairs={{0,2},{2,4},{4,6},{6,8},{8,10},{10,12},{12,14},{14,16},{16,18},{18... | collective-permute-start | bytes 3080 | tf_op jit(solution)/shard_map/ppermute | solution.py:22
  46.1 6.0 %collective-permute-start.8 = (bf16[256,64]{0,1:T(8,128)(2,1)}, bf16[256,64]{0,1:T(8,128)(2,1)S(1)}, u32[]{:S(2)}, u32[]{:S(2)}) collective-permute-start(bf16[256,64]{0,1:T(8,128)(2,1)} %param.17), channel_id=1, source_target_pairs={{0,8},{2,10},{4,12},{6,14},{8,16},{10,18},{12,20},{14,22},{16,24},... | collective-permute-start | bytes 98312 | tf_op jit(solution)/shard_map/ppermute | solution.py:22
  52.1 6.9 %collective-permute-start.9 = (bf16[256,64]{0,1:T(8,128)(2,1)}, bf16[256,64]{0,1:T(8,128)(2,1)S(1)}, u32[]{:S(2)}, u32[]{:S(2)}) collective-permute-start(bf16[256,64]{0,1:T(8,128)(2,1)} %param.17), channel_id=1, source_target_pairs={{0,6},{2,8},{4,10},{6,12},{8,14},{10,16},{12,18},{14,20},{16,22},{... | collective-permute-start | bytes 98312 | tf_op jit(solution)/shard_map/ppermute | solution.py:22
  59.0 6.9 %collective-permute-start.10 = (bf16[256,64]{0,1:T(8,128)(2,1)}, bf16[256,64]{0,1:T(8,128)(2,1)S(1)}, u32[]{:S(2)}, u32[]{:S(2)}) collective-permute-start(bf16[256,64]{0,1:T(8,128)(2,1)} %param.17), channel_id=1, source_target_pairs={{0,4},{2,6},{4,8},{6,10},{8,12},{10,14},{12,16},{14,18},{16,20},{1... | collective-permute-start | bytes 98312 | tf_op jit(solution)/shard_map/ppermute | solution.py:22
  65.9 7.8 %collective-permute-start.11 = (bf16[256,64]{0,1:T(8,128)(2,1)}, bf16[256,64]{0,1:T(8,128)(2,1)S(1)}, u32[]{:S(2)}, u32[]{:S(2)}) collective-permute-start(bf16[256,64]{0,1:T(8,128)(2,1)} %param.17), channel_id=1, source_target_pairs={{0,2},{2,4},{4,6},{6,8},{8,10},{10,12},{12,14},{14,16},{16,18},{18... | collective-permute-start | bytes 98312 | tf_op jit(solution)/shard_map/ppermute | solution.py:22
  79.7 2.3 copy-start.2
  82.0 1.0 copy-start.5
  83.6 9.0 %copy-start.6 = (s32[128,2]{0,1:T(2,128)S(1)}, s32[128,2]{0,1:T(2,128)}, u32[]{:S(2)}) copy-start(s32[128,2]{0,1:T(2,128)} %param.26) | copy-start | bytes 3076
  89.9 9.8 %copy-start.3 = (bf16[128,2048]{1,0:T(8,128)(2,1)S(1)}, bf16[128,2048]{1,0:T(8,128)(2,1)}, u32[]{:S(2)}) copy-start(bf16[128,2048]{1,0:T(8,128)(2,1)} %param.24) | copy-start | bytes 1572868
  89.9 12.5 %copy-start.7 = (f32[2048]{0:T(1024)S(1)}, f32[2048]{0:T(1024)}, u32[]{:S(2)}) copy-start(f32[2048]{0:T(1024)} %param.25) | copy-start | bytes 24580
  92.6 79.8 %all-gather.3.cloned.1.call-start = ((), (), s32[]{:S(2)}) async-start(), calls=%async_computation.4 | async-start | bytes 6291456 | tf_op jit(solution)/shard_map/all_gather | solution.py:141
  158.4 82.8 %all-reduce.3.cloned.1.call-start = ((), (), s32[]{:S(2)}) async-start(), calls=%async_computation.5 | async-start | bytes 8388608
  185.9 25.9 %copy-start.10 = (u32[32]{0:T(128)S(1)}, u32[32]{0:T(128)}, u32[]{:S(2)}) copy-start(u32[32]{0:T(128)} %constant.72) | copy-start | bytes 388
  211.8 40.6 %copy-start.9 = (f32[128,2]{0,1:T(2,128)S(1)}, f32[128,2]{0,1:T(2,128)}, u32[]{:S(2)}) copy-start(f32[128,2]{0,1:T(2,128)} %param.27) | copy-start | bytes 3076
  245.0 55.6 %all-to-all-start.1 = ((bf16[16,32,2048]{2,1,0:T(8,128)(2,1)}), bf16[16,32,2048]{2,1,0:T(8,128)(2,1)}, u32[]{:S(2)}, u32[]{:S(2)}) async-start(bf16[16,32,2048]{2,1,0:T(8,128)(2,1)} %dynamic-slice_bitcast_fusion), calls=%async_computation.2 | async-start | bytes 4194304 | tf_op jit(solution)/shard_map/all_to_all | solution.py:155
  300.6 15.0 %copy-start.1 = (bf16[512,2048]{1,0:T(8,128)(2,1)S(1)}, bf16[512,2048]{1,0:T(8,128)(2,1)}, u32[]{:S(2)}) copy-start(bf16[512,2048]{1,0:T(8,128)(2,1)} %param.23) | copy-start | bytes 6291460
  305.9 8.6 %copy-start.8 = (f32[2048]{0:T(1024)S(1)}, f32[2048]{0:T(1024)}, u32[]{:S(2)}) copy-start(f32[2048]{0:T(1024)} %param.31) | copy-start | bytes 24580
Sparse Core Ops, SparseCore 0:
  92.8 6.8 reduce-scatter.4
  158.5 13.8 all-gather.2
  211.9 29.2 all-reduce.2
where the time goes:
time: 323 us; the launch traced here: 322 us
  waiting for transfers between devices  126 us (39%)
  blocking collectives  54 us (17%)
  matrix products  52.9 us (16%)
  starting transfers between devices  40.9 us (13%)
  local copies, waits for them, and re-layouts  19.4 us (6%)
  other arithmetic  15.7 us (5%)
  between operations  13.6 us (4%)
    all_to_all x1, blocking collectives, per_device(): lax.all_to_all(outbound, 'sp', split_axis=0, concat_axis=0, tiled=True)  54 us
    all_to_all x1, waiting for transfers between devices, per_device(): lax.all_to_all(reduced.reshape(chip_count, capacity, model_width), 'sp',...  48.1 us
    ppermute x12, starting transfers between devices, shifted(): lax.ppermute(value, axis, [(source, source + steps) for source in range(l...  33.7 us
    ppermute x12, waiting for transfers between devices, shifted(): lax.ppermute(value, axis, [(source, source + steps) for source in range(l...  29.6 us
    unnamed x4, waiting for transfers between devices  28.9 us
    dot_general x1, matrix products, per_device(): jnp.dot(hidden, w_down[0], preferred_element_type=jnp.float32)  25.8 us
    all_gather x1, waiting for transfers between devices, per_device(): arrived = lax.all_gather(landed[:, None], 'tp', axis=1, tiled=True)  13.8 us
    dot_general x1, matrix products, per_device(): gate_pre = jnp.dot(flat_rows, w_gate[0], preferred_element_type=jnp.float32)  13.5 us
  transfers between devices with their start and end apart: 16, of which 12 were waited for; matrix products, arithmetic and copies ran while one was open for 2% of the time, Pallas kernels for 0%

commit v1 on v0

v1 whole, which is shorter than its diff:
```python
import functools

import jax
import jax.numpy as jnp
import numpy as np
from jax import lax
from jax.experimental import pallas as pl
from jax.experimental.pallas import tpu as pltpu
from jax.sharding import PartitionSpec as P


HEADS = 8
DK = 128
DR = 64
DV = 128
TOPK = 2
REACH = 4

ROPE_THETA = 500000.0
RESIDUAL_SCALE = 2.0**0.5
NORM_EPSILON = 1e-05
LANES = 128
FAR = 2.0**24
F32 = jnp.float32
BF16 = jnp.bfloat16


def dot(a, b, dims=((1,), (0,))):
    return lax.dot_general(a, b, (dims, ((), ())), preferred_element_type=F32)


def iota(shape, axis):
    return lax.broadcasted_iota(jnp.int32, shape, axis)


def call(body, outs, args, flops, limit=12, scalars=0, hbm=(), scratch=()):
    specs = [
        pl.BlockSpec(memory_space=pltpu.SMEM)
        if k < scalars
        else pl.BlockSpec(memory_space=pl.ANY if k in hbm else pltpu.VMEM)
        for k in range(len(args))
    ]
    return pl.pallas_call(
        body,
        out_shape=outs,
        in_specs=specs,
        out_specs=jax.tree.map(lambda _: pl.BlockSpec(memory_space=pltpu.VMEM), outs),
        scratch_shapes=list(scratch),
        cost_estimate=pl.CostEstimate(flops=flops, bytes_accessed=1 << 20, transcendentals=0),
        compiler_params=pltpu.CompilerParams(vmem_limit_bytes=limit * 2**20),
    )(*args)


def far(value):
    return pltpu.with_memory_space_constraint(value, pltpu.HBM)


def shape(*dims, dtype=BF16):
    return jax.ShapeDtypeStruct(dims, dtype)


def angle_tables(tok_dev, chips):
    half = DR // 2
    frequency = ROPE_THETA ** (-2.0 * np.arange(half) / DR)
    lanes = frequency[np.arange(LANES) % half]
    near = np.arange(tok_dev)[:, None] * lanes[None, :]
    base = (np.arange(chips) * tok_dev)[:, None] * lanes[None, :]
    return [np.asarray(t, np.float32) for t in (np.cos(near), np.sin(near), np.cos(base), np.sin(base))]


def turn_tables(sp, rows, near_cos, near_sin, base_cos, base_sin):
    cb, sb = base_cos[pl.ds(sp, 1), :], base_sin[pl.ds(sp, 1), :]
    cn, sn = near_cos[rows, :], near_sin[rows, :]
    sine = sb * cn + cb * sn
    low = (iota(sine.shape, 1) % DR) < DR // 2
    return cb * cn - sb * sn, jnp.where(low, -sine, sine)


def pack_kernel(where, latent, rotary, docs, nc, ns, bc, bs, own, send):
    sp, tp = where[0], where[1]
    rows = latent.shape[0]
    cosine, sine = turn_tables(sp, slice(None), nc, ns, bc, bs)
    a, b = iota((DR, LANES), 0), iota((DR, LANES), 1)
    keep = (a == b).astype(BF16)
    swap = ((a == (b ^ (DR // 2))) & (b < DR)).astype(BF16)
    turned = dot(rotary[...], keep, ((0,), (0,))) * cosine
    turned = turned + dot(rotary[...], swap, ((0,), (0,))) * sine
    marks = (iota((LANES - DR, rows), 0) == docs[...]).astype(BF16)
    shift = (a == b - DR).astype(BF16)
    turned = turned + dot(marks, shift, ((0,), (0,)))
    width = latent.shape[1]
    own[:, :width] = latent[...]
    own[:, width:] = turned.astype(BF16)
    half = send.shape[0]
    part = pl.ds(pl.multiple_of(tp * half, half), half)
    send[...] = own[part, :]


def ready_kernel(where, content, content_far, turning, turning_far, docs, routes, nc, ns, bc, bs, queries, pick0, pick1, *, capacity):
    sp, tp = where[0], where[1]
    rows = content.shape[0]
    heads_here = HEADS // 2
    part = pl.ds(pl.multiple_of(tp * rows, rows), rows)
    cosine, sine = turn_tables(sp, part, nc, ns, bc, bs)
    a, b = iota((LANES, LANES), 0), iota((LANES, LANES), 1)
    swap = (a == (b ^ (DR // 2))).astype(BF16)
    marks = (iota((LANES - DR, rows), 0) == docs[:, part]).astype(BF16)
    a, b = iota((DR, LANES), 0), iota((DR, LANES), 1)
    same = dot(marks, (a == b - DR).astype(BF16), ((0,), (0,)))
    lane = iota((rows, LANES), 1)
    barred = (same - 1.0) * FAR
    for group, (plain, spun) in enumerate(((content, turning), (content_far, turning_far))):
        for pair in range(heads_here // 2):
            raw = spun[:, pair * LANES : (pair + 1) * LANES]
            turned = raw.astype(F32) * cosine + dot(raw, swap) * sine
            for side in range(2):
                head = group * heads_here + pair * 2 + side
                local = pair * 2 + side
                queries[:, head * 256 : head * 256 + DK] = plain[:, local * DK : (local + 1) * DK]
                value = turned if side == 0 else pltpu.roll(turned, DR, 1)
                queries[:, head * 256 + DK : head * 256 + 256] = jnp.where(
                    lane < DR, value, barred
                ).astype(BF16)
    slots = pick0.shape[1]
    spread = (iota((TOPK, LANES), 0) == iota((TOPK, LANES), 1)).astype(BF16)
    turned = dot(routes[...].astype(F32).astype(BF16), spread, ((0,), (0,))).astype(jnp.int32)
    first, second = turned[:, 0:1], turned[:, 1:2]
    member = ((first == lane) | (second == lane)).astype(BF16)
    earlier = (iota((rows, rows), 0) > iota((rows, rows), 1)).astype(BF16)
    rank = dot(earlier, member)
    slot = iota((rows, slots), 1)
    for route, pick in ((first, pick0), (second, pick1)):
        place = jnp.sum(jnp.where(route == lane, rank, 0.0), 1, keepdims=True).astype(jnp.int32)
        pick[...] = (slot == (route ^ sp) * capacity + place).astype(BF16)


def layer_norm(values, gain):
    centre = jnp.mean(values, -1, keepdims=True)
    moved = values - centre
    spread = jnp.mean(jnp.square(moved), -1, keepdims=True)
    return moved * lax.rsqrt(spread + NORM_EPSILON) * gain


def attend_kernel(where, *refs, near, pieces, capacity):
    kv_own, kv_near = refs[0], refs[1 : 1 + near]
    queries, key_up, value_up, out_mine, out_theirs, residual, gain, pick0, pick1, down = refs[
        1 + near : 11 + near
    ]
    normed, down_held = refs[11 + near : 13 + near]
    outbound = refs[13 + near : 13 + near + pieces]
    packed, keys, values, attended, summed, w_mine, w_theirs, sems = refs[13 + near + pieces :]
    tp = where[1]
    copies = [
        pltpu.make_async_copy(out_mine, w_mine, sems.at[0]),
        pltpu.make_async_copy(out_theirs, w_theirs, sems.at[1]),
        pltpu.make_async_copy(down, down_held, sems.at[2]),
    ]
    for copy in copies:
        copy.start()
    own_rows = kv_own.shape[0]
    packed[:own_rows, :] = kv_own[...]
    at = own_rows
    for ref in kv_near:
        packed[at : at + ref.shape[0], :] = ref[...]
        at += ref.shape[0]
    rank = key_up.shape[0]
    latent = packed[:, :rank]
    keys[...] = dot(latent, key_up[...]).astype(BF16)
    values[...] = dot(latent, value_up[...]).astype(BF16)
    rows = queries.shape[0]
    scale = (DK + DR) ** -0.5
    ahead = iota((rows, own_rows), 1) > iota((rows, own_rows), 0) + tp * rows

    def head_step(head, carry):
        column = lax.rem(tp * (HEADS // 2) + head, HEADS) * DK
        cols = pl.ds(pl.multiple_of(column, LANES), DK)
        query = queries[:, pl.ds(pl.multiple_of(head * 256, 256), 256)]
        key = jnp.concatenate([keys[:, cols], packed[:, rank:]], 1)
        scores = dot(query, key, ((1,), (1,)))
        scores = jnp.concatenate(
            [jnp.where(ahead, -FAR, scores[:, :own_rows]), scores[:, own_rows:]], 1
        )
        peak = jnp.max(scores, -1, keepdims=True)
        lifted = jnp.exp((scores - peak) * scale)
        total = jnp.sum(lifted, -1, keepdims=True)
        mixed = dot(lifted.astype(BF16), values[:, cols]) / total
        attended[:, pl.ds(pl.multiple_of(head * DV, LANES), DV)] = mixed.astype(BF16)
        return carry

    lax.fori_loop(0, HEADS, head_step, 0)
    half = w_mine.shape[0]
    copies[0].wait()
    summed[...] = dot(attended[:, :half], w_mine[...]).astype(BF16).astype(F32)
    copies[1].wait()
    summed[...] += dot(attended[:, half:], w_theirs[...]).astype(BF16).astype(F32)
    step = 32

    def norm_step(k, carry):
        part = pl.ds(pl.multiple_of(k * step, step), step)
        value = RESIDUAL_SCALE * residual[part, :].astype(F32) + summed[part, :]
        normed[part, :] = layer_norm(value, gain[...]).astype(BF16)
        return carry

    lax.fori_loop(0, rows // step, norm_step, 0)
    both = pick0[...] + pick1[...]
    placed = dot(both, normed[...], ((0,), (0,))).astype(BF16)
    for k, ref in enumerate(outbound):
        ref[...] = placed[k * capacity : (k + 1) * capacity]
    copies[2].wait()


def expert_kernel(own, other, w_gate, w_up, w_down, mine, theirs, rows_in, hidden, *, tile):
    half = own.shape[0]
    rows_in[:half, :] = own[...]
    rows_in[half:, :] = other[...]

    def hidden_step(step, carry):
        cols = pl.ds(pl.multiple_of(step * tile, tile), tile)
        value = rows_in[...]
        gate = dot(value, w_gate[0, :, cols])
        upward = dot(value, w_up[0, :, cols])
        hidden[:, cols] = (gate / (1.0 + jnp.exp(-gate)) * upward).astype(BF16)
        return carry

    lax.fori_loop(0, hidden.shape[1] // tile, hidden_step, 0)

    def down_step(step, carry):
        cols = pl.ds(pl.multiple_of(step * tile, tile), tile)
        partial = dot(hidden[...], w_down[0, :, cols]).astype(BF16)
        mine[:, cols] = partial[:half]
        theirs[:, cols] = partial[half:]
        return carry

    lax.fori_loop(0, mine.shape[1] // tile, down_step, 0)


def experts(own, other, w_gate, w_up, w_down):
    half, width = own.shape
    hidden = w_gate.shape[2]
    rows = 2 * half
    return call(
        functools.partial(expert_kernel, tile=256),
        [shape(half, width)] * 2,
        [own, other, w_gate, w_up, w_down],
        6 * rows * width * hidden,
        limit=14,
        scratch=[pltpu.VMEM((rows, width), BF16), pltpu.VMEM((rows, hidden), BF16)],
    )


def add_kernel(a, b, *outs):
    capacity = outs[0].shape[0]
    for k, ref in enumerate(outs):
        part = slice(k * capacity, (k + 1) * capacity)
        ref[...] = (a[part, :].astype(F32) + b[part, :].astype(F32)).astype(BF16)


def pick_rows(pick0, pick1, weights, refs, stacked, summed, pieces, capacity):
    for k, ref in enumerate(refs):
        stacked[k * capacity : (k + 1) * capacity, :] = ref[...]
    rows = pick0.shape[0]
    chosen = [
        jnp.concatenate([pick[:, s * capacity : (s + 1) * capacity] for s in pieces], 1)
        for pick in (pick0, pick1)
    ]
    summed[...] = dot(jnp.concatenate(chosen, 0), stacked[...])
    spread = (iota((TOPK, LANES), 0) == iota((TOPK, LANES), 1)).astype(F32)
    weight = lax.dot_general(
        weights[...],
        spread,
        (((0,), (0,)), ((), ())),
        precision=lax.Precision.HIGHEST,
        preferred_element_type=F32,
    )
    return weight[:, 0:1], weight[:, 1:2], rows


def early_kernel(normed, pick0, pick1, weights, *refs, pieces, capacity):
    out, stacked, summed = refs[-3:]
    first, second, rows = pick_rows(pick0, pick1, weights, refs[:-3], stacked, summed, pieces, capacity)
    out[...] = RESIDUAL_SCALE * normed[...].astype(F32) + (
        summed[:rows, :] * first + summed[rows:, :] * second
    )


def final_kernel(begun, pick0, pick1, weights, gain, *refs, pieces, capacity):
    out, stacked, summed = refs[-3:]
    first, second, rows = pick_rows(pick0, pick1, weights, refs[:-3], stacked, summed, pieces, capacity)
    step = 32
    for k in range(rows // step):
        part, lower = slice(k * step, (k + 1) * step), slice(rows + k * step, rows + (k + 1) * step)
        value = begun[part, :] + (summed[part, :] * first[part] + summed[lower, :] * second[part])
        out[part, :] = layer_norm(value, gain[...]).astype(BF16)


def group_order(chips):
    order = np.arange(chips).reshape(4, chips // 4)
    half = chips // 8
    groups = [order[2:, :half], order[2:, half:], order[1], order[0]]
    return [[int(s) for s in group.reshape(-1)] for group in groups]


def per_device(
    latent,
    rotary_key,
    doc_ids,
    queries_content,
    queries_rotary,
    w_key_up,
    w_value_up,
    w_out,
    residual,
    norm_gain,
    routes,
    route_weights,
    w_gate,
    w_up,
    w_down,
    out_gain,
):
    tok_dev = latent.shape[0]
    chips = lax.axis_size("sp")
    rows, width = residual.shape
    capacity = max(2, 2 * rows * TOPK // chips)
    sp, tp = lax.axis_index("sp"), lax.axis_index("tp")
    where = jnp.stack([sp, tp]).astype(jnp.int32)
    tables = angle_tables(tok_dev, chips)
    docs = doc_ids.reshape(1, tok_dev)

    def across(value):
        return lax.ppermute(value, "tp", [(0, 1), (1, 0)])

    def exchange(value, s):
        if s == 0:
            return value
        return lax.ppermute(value, "sp", [(j, j ^ s) for j in range(chips)])

    packed_width = latent.shape[1] + LANES
    kv_own, kv_send = call(
        pack_kernel,
        [shape(tok_dev, packed_width), shape(rows, packed_width)],
        [where, far(latent), far(rotary_key.T), far(docs), *map(far, tables)],
        1 << 26,
        scalars=1,
    )
    kv_near = [
        lax.ppermute(kv_send, "sp", [(j, (j + d) % chips) for j in range(chips)])
        for d in range(REACH, 0, -1)
    ]
    out_theirs = across(w_out)
    queries_content, queries_rotary, _ = lax.optimization_barrier(
        (queries_content, queries_rotary, kv_send)
    )

    def split(value):
        mine = lax.dynamic_slice_in_dim(value, tp * rows, rows, 0)
        return mine, across(lax.dynamic_slice_in_dim(value, (1 - tp) * rows, rows, 0))

    queries_ready, pick0, pick1 = call(
        functools.partial(ready_kernel, capacity=capacity),
        [shape(rows, HEADS * 256), shape(rows, chips * capacity), shape(rows, chips * capacity)],
        [where, *split(queries_content), *split(queries_rotary), far(docs), far(routes.T), *map(far, tables)],
        1 << 26,
        scalars=1,
    )
    kv_near, queries_ready = lax.optimization_barrier((kv_near, queries_ready))
    kv_all = [jnp.concatenate(kv_near, 0)]
    kv_all.append(across(kv_all[0]))
    reach = tok_dev + sum(value.shape[0] for value in kv_all)
    args = [where, kv_own, *kv_all, queries_ready, far(w_key_up), far(w_value_up), far(w_out), out_theirs]
    hbm = (len(args) - 2, len(args) - 1, len(args) + 4)
    args += [far(residual), far(norm_gain.reshape(1, width)), pick0, pick1, far(w_down)]
    normed, w_down, *outbound = call(
        functools.partial(attend_kernel, near=len(kv_all), pieces=chips, capacity=capacity),
        [shape(rows, width), shape(*w_down.shape)] + [shape(capacity, width)] * chips,
        args,
        1 << 32,
        limit=34,
        scalars=1,
        hbm=hbm,
        scratch=[
            pltpu.VMEM((reach, packed_width), BF16),
            pltpu.VMEM((reach, HEADS * DK), BF16),
            pltpu.VMEM((reach, HEADS * DV), BF16),
            pltpu.VMEM((rows, HEADS * DV), BF16),
            pltpu.VMEM((rows, width), F32),
            pltpu.VMEM(w_out.shape, BF16),
            pltpu.VMEM(w_out.shape, BF16),
            pltpu.SemaphoreType.DMA((3,)),
        ],
    )
    groups = group_order(chips)
    w_gate, w_up, w_down = (
        pltpu.with_memory_space_constraint(w, pltpu.VMEM) for w in (w_gate, w_up, w_down)
    )
    landed, returned, done = {}, {}, {}
    for number in (0, 2, 3, 1):
        for s in groups[number]:
            landed[s] = exchange(outbound[s], s)
    after = ()
    for number in (0, 2, 1, 3):
        group = groups[number]
        own = jnp.concatenate([landed[s] for s in group], 0)
        other = across(own)
        own, other, _ = lax.optimization_barrier((own, other, after))
        mine, theirs = experts(own, other, w_gate, w_up, w_down)
        after = (mine, done.get(0, ()), done.get(1, ()))
        done[number] = call(
            add_kernel, [shape(capacity, width)] * len(group), [mine, across(theirs)], 1 << 20
        )
        for s, value in zip(group, done[number]):
            returned[s] = exchange(value, s)
    early, late = groups[0] + groups[2] + groups[3], groups[1]

    def gathered(total, pieces, body, out, extra=()):
        return call(
            functools.partial(body, pieces=pieces, capacity=capacity),
            out,
            [total, pick0, pick1, route_weights.T, *extra, *[returned[s] for s in pieces]],
            4 * rows * len(pieces) * capacity * width,
            limit=16,
            scratch=[
                pltpu.VMEM((len(pieces) * capacity, width), BF16),
                pltpu.VMEM((TOPK * rows, width), F32),
            ],
        )

    begun = gathered(normed, early, early_kernel, shape(rows, width, dtype=F32))
    return gathered(begun, late, final_kernel, shape(rows, width), [out_gain.reshape(1, width)])


def solution(mesh):
    return jax.shard_map(
        per_device,
        mesh=mesh,
        in_specs=(
            P("sp", None),
            P("sp", None),
            P("sp"),
            P("sp", "tp"),
            P("sp", "tp"),
            P(),
            P(),
            P("tp", None),
            P(("sp", "tp"), None),
            P(),
            P(("sp", "tp"), None),
            P(("sp", "tp"), None),
            P("sp", None, "tp"),
            P("sp", None, "tp"),
            P("sp", "tp", None),
            P(),
        ),
        out_specs=P(("sp", "tp"), None),
        check_vma=False,
    )
```

time: 323 us -> 197 us (0.61)
  blocking collectives: 54 us -> 0 us
  Pallas kernels: 0 us -> 53.9 us
  matrix products: 52.9 us -> 0 us
  waiting for transfers between devices: 126 us -> 74 us
  starting transfers between devices: 40.9 us -> 66.1 us
  local copies, waits for them, and re-layouts: 19.4 us -> 2.13 us
  other arithmetic: 15.7 us -> 0.08 us
  between operations: 13.6 us -> 0.41 us
    all_to_all x1 -> x0, blocking collectives: 54 us -> none  [per_device(): lax.all_to_all(outbound, 'sp', split_axis=0, concat_axis=0, tiled=True)]
    pallas_call x0 -> x13, Pallas kernels: none -> 53.9 us  [call(): pl.pallas_call(body, out_shape=outs, in_specs=specs, out_specs=jax.tree.m...]
    dot_general x9 -> x0, matrix products: 52.9 us -> none  [the longest x1 25.8 us: per_device(): jnp.dot(hidden, w_down[0], preferred_element_type=jnp.float32)]
    all_to_all x1 -> x0, waiting for transfers between devices: 48.1 us -> none  [per_device(): lax.all_to_all(reduced.reshape(chip_count, capacity, model_width), 'sp',...]
    ppermute x12 -> x46, waiting for transfers between devices: 29.6 us -> 74 us  [the longest x30 69.5 us: exchange(): return lax.ppermute(value, 'sp', [(j, j ^ s) for j in range(chips)])]
    ppermute x12 -> x46, starting transfers between devices: 33.7 us -> 66.1 us  [the longest x30 57.6 us: exchange(): return lax.ppermute(value, 'sp', [(j, j ^ s) for j in range(chips)])]
    unnamed x4 -> x0, waiting for transfers between devices: 28.9 us -> none
    all_gather x1 -> x0, waiting for transfers between devices: 13.8 us -> none  [per_device(): arrived = lax.all_gather(landed[:, None], 'tp', axis=1, tiled=True)]
  transfers between devices with their start and end apart: 16 -> 46, of which waited for: 12 -> 22; matrix products, arithmetic and copies ran while one was open for 2% -> 1% of each run, Pallas kernels for 0% -> 20%
where the time goes in v1:
time: 197 us
  waiting for transfers between devices  74 us (38%)
  starting transfers between devices  66.1 us (34%)
  Pallas kernels  53.9 us (27%)
  local copies, waits for them, and re-layouts  2.13 us (1%)
    ppermute x30, waiting for transfers between devices, exchange(): return lax.ppermute(value, 'sp', [(j, j ^ s) for j in range(chips)])  69.5 us
    ppermute x30, starting transfers between devices, exchange(): return lax.ppermute(value, 'sp', [(j, j ^ s) for j in range(chips)])  57.6 us
    pallas_call x13, Pallas kernels, call(): pl.pallas_call(body, out_shape=outs, in_specs=specs, out_specs=jax.tree.m...  53.9 us
    ppermute x4, starting transfers between devices, per_device(): lax.ppermute(kv_send, 'sp', [(j, (j + d) % chips) for j in range(chips)])  5.72 us
  transfers between devices with their start and end apart: 46, of which 22 were waited for; matrix products, arithmetic and copies ran while one was open for 1% of the time, Pallas kernels for 20%

profile of v1, /device:TPU:16, one launch (start us, length us, event | category | flops | bytes accessed | tf_op | source)
XLA Modules:
  0.0 196.6 jit_solution(422401259969069397)
XLA Ops:
  7.0 2.4 %collective-permute-start.1 = (bf16[128,384]{1,0:T(8,128)(2,1)S(1)}, bf16[128,384]{1,0:T(8,128)(2,1)S(1)}, u32[]{:S(2)}, u32[]{:S(2)}) collective-permute-start(bf16[128,384]{1,0:T(8,128)(2,1)S(1)} %get-tuple-element.68), channel_id=1, source_target_pairs={{0,6},{2,8},{4,10},{6,12},{8,14},{10,16},{12,18},{14,20},{16,22},{... | collective-permute-start | bytes 294920 | tf_op jit(solution)/shard_map/ppermute | solution.py:347
  16.0 12.4 %shard_map.192 = (bf16[128,2048]{1,0:T(8,128)(2,1)S(1)}, bf16[1,1792,2048]{2,1,0:T(8,128)(2,1)S(1)}, bf16[32,2048]{1,0:T(8,128)(2,1)S(1)}, bf16[32,2048]{1,0:T(8...) custom-call(s32[2]{0:T(128)S(1)} %pad_add_fusion.where, ...), custom_call_target="tpu_custom_call" | custom-call | flops 4294967296 | bytes 1048576 | tf_op jit(solution)/shard_map/pallas_call | solution.py:43
  30.6 2.4 %collective-permute-start.9 = (bf16[32,2048]{1,0:T(8,128)(2,1)S(1)}, bf16[32,2048]{1,0:T(8,128)(2,1)S(1)}, u32[]{:S(2)}, u32[]{:S(2)}) collective-permute-start(bf16[32,2048]{1,0:T(8,128)(2,1)S(1)} %get-tuple-element.81), channel_id=1, source_target_pairs={{0,18},{2,16},{4,22},{6,20},{8,26},{10,24},{12,30},{14,28},{16,2},... | collective-permute-start | bytes 393224 | tf_op jit(solution)/shard_map/ppermute | solution.py:336
  34.9 5.8 %collective-permute-start.32 = (bf16[32,2048]{1,0:T(8,128)(2,1)S(1)}, bf16[32,2048]{1,0:T(8,128)(2,1)S(1)}, u32[]{:S(2)}, u32[]{:S(2)}) collective-permute-start(bf16[32,2048]{1,0:T(8,128)(2,1)S(1)} %get-tuple-element.109), channel_id=1, source_target_pairs={{0,20},{2,22},{4,16},{6,18},{8,28},{10,30},{12,24},{14,26},{16,4},... | collective-permute-start | bytes 393224 | tf_op jit(solution)/shard_map/ppermute | solution.py:336
  40.8 16.8 %collective-permute-done.32 = bf16[32,2048]{1,0:T(8,128)(2,1)S(1)} collective-permute-done((bf16[32,2048]{1,0:T(8,128)(2,1)S(1)}, bf16[32,2048]{1,0:T(8,128)(2,1)S(1)}, u32[]{:S(2)}, u32[]{:S(2)}) %collective-permute-start.32) | collective-permute-done | bytes 131104 | tf_op jit(solution)/shard_map/ppermute | solution.py:336
  57.6 5.3 %collective-permute-start.18 = (bf16[32,2048]{1,0:T(8,128)(2,1)S(1)}, bf16[32,2048]{1,0:T(8,128)(2,1)S(1)}, u32[]{:S(2)}, u32[]{:S(2)}) collective-permute-start(bf16[32,2048]{1,0:T(8,128)(2,1)S(1)} %get-tuple-element.93), channel_id=1, source_target_pairs={{0,8},{2,10},{4,12},{6,14},{8,0},{10,2},{12,4},{14,6},{16,24},{18,... | collective-permute-start | bytes 393224 | tf_op jit(solution)/shard_map/ppermute | solution.py:336
  63.0 3.5 %collective-permute-done.18 = bf16[32,2048]{1,0:T(8,128)(2,1)S(1)} collective-permute-done((bf16[32,2048]{1,0:T(8,128)(2,1)S(1)}, bf16[32,2048]{1,0:T(8,128)(2,1)S(1)}, u32[]{:S(2)}, u32[]{:S(2)}) %collective-permute-start.18) | collective-permute-done | bytes 131104 | tf_op jit(solution)/shard_map/ppermute | solution.py:336
  66.4 3.3 %collective-permute-start.19 = (bf16[32,2048]{1,0:T(8,128)(2,1)S(1)}, bf16[32,2048]{1,0:T(8,128)(2,1)S(1)}, u32[]{:S(2)}, u32[]{:S(2)}) collective-permute-start(bf16[32,2048]{1,0:T(8,128)(2,1)S(1)} %get-tuple-element.94), channel_id=1, source_target_pairs={{0,10},{2,8},{4,14},{6,12},{8,2},{10,0},{12,6},{14,4},{16,26},{18,... | collective-permute-start | bytes 393224 | tf_op jit(solution)/shard_map/ppermute | solution.py:336
  69.8 4.1 %collective-permute-done.19 = bf16[32,2048]{1,0:T(8,128)(2,1)S(1)} collective-permute-done((bf16[32,2048]{1,0:T(8,128)(2,1)S(1)}, bf16[32,2048]{1,0:T(8,128)(2,1)S(1)}, u32[]{:S(2)}, u32[]{:S(2)}) %collective-permute-start.19) | collective-permute-done | bytes 131104 | tf_op jit(solution)/shard_map/ppermute | solution.py:336
  76.1 2.8 %collective-permute-start.29 = (bf16[32,2048]{1,0:T(8,128)(2,1)S(1)}, bf16[32,2048]{1,0:T(8,128)(2,1)S(1)}, u32[]{:S(2)}, u32[]{:S(2)}) collective-permute-start(bf16[32,2048]{1,0:T(8,128)(2,1)S(1)} %get-tuple-element.107), channel_id=1, source_target_pairs={{0,4},{2,6},{4,0},{6,2},{8,12},{10,14},{12,8},{14,10},{16,20},{18,... | collective-permute-start | bytes 393224 | tf_op jit(solution)/shard_map/ppermute | solution.py:336
  82.4 2.8 %collective-permute-start.33 = (bf16[32,2048]{1,0:T(8,128)(2,1)S(1)}, bf16[32,2048]{1,0:T(8,128)(2,1)S(1)}, u32[]{:S(2)}, u32[]{:S(2)}) collective-permute-start(bf16[32,2048]{1,0:T(8,128)(2,1)S(1)} %get-tuple-element.110), channel_id=1, source_target_pairs={{0,22},{2,20},{4,18},{6,16},{8,30},{10,28},{12,26},{14,24},{16,6},... | collective-permute-start | bytes 393224 | tf_op jit(solution)/shard_map/ppermute | solution.py:336
  85.3 3.1 %collective-permute-start.34 = (bf16[32,2048]{1,0:T(8,128)(2,1)S(1)}, bf16[32,2048]{1,0:T(8,128)(2,1)S(1)}, u32[]{:S(2)}, u32[]{:S(2)}) collective-permute-start(bf16[32,2048]{1,0:T(8,128)(2,1)S(1)} %get-tuple-element.111), channel_id=1, source_target_pairs={{0,28},{2,30},{4,24},{6,26},{8,20},{10,22},{12,16},{14,18},{16,12}... | collective-permute-start | bytes 393224 | tf_op jit(solution)/shard_map/ppermute | solution.py:336
  89.9 4.8 %collective-permute-done.33 = bf16[32,2048]{1,0:T(8,128)(2,1)S(1)} collective-permute-done((bf16[32,2048]{1,0:T(8,128)(2,1)S(1)}, bf16[32,2048]{1,0:T(8,128)(2,1)S(1)}, u32[]{:S(2)}, u32[]{:S(2)}) %collective-permute-start.33) | collective-permute-done | bytes 131104 | tf_op jit(solution)/shard_map/ppermute | solution.py:336
  94.7 4.5 %collective-permute-done.34 = bf16[32,2048]{1,0:T(8,128)(2,1)S(1)} collective-permute-done((bf16[32,2048]{1,0:T(8,128)(2,1)S(1)}, bf16[32,2048]{1,0:T(8,128)(2,1)S(1)}, u32[]{:S(2)}, u32[]{:S(2)}) %collective-permute-start.34) | collective-permute-done | bytes 131104 | tf_op jit(solution)/shard_map/ppermute | solution.py:336
  101.0 8.7 %shard_map.193 = (bf16[128,2048]{1,0:T(8,128)(2,1)S(1)}, bf16[128,2048]{1,0:T(8,128)(2,1)S(1)}) custom-call(bf16[128,2048]{1,0:T(8,128)(2,1)S(1)} %constant_dynamic-update-slice_fusion.4.own, bf16[128,2048]{1,0:T(8,128)(2,1)S(1)} %collective-permute-done.12.other, bf16[1,2048,1792]{2,1,0:T(8,128)(2,1)S(1)} %bitcast.9, bf16[1,2048,1792]{2,1,0:T(8,128)(2,1)S(1)} %bitcast.11, ...), custom_call_target="tpu_custom_call" | custom-call | flops 5637144576 | bytes 1048576 | tf_op jit(solution)/shard_map/pallas_call | solution.py:43
  110.3 8.7 %shard_map.195 = (bf16[128,2048]{1,0:T(8,128)(2,1)S(1)}, bf16[128,2048]{1,0:T(8,128)(2,1)S(1)}) custom-call(bf16[128,2048]{1,0:T(8,128)(2,1)S(1)} %constant_dynamic-update-slice_fusion.8.own, bf16[128,2048]{1,0:T(8,128)(2,1)S(1)} %collective-permute-done.22.other, bf16[1,2048,1792]{2,1,0:T(8,128)(2,1)S(1)} %bitcast.9, bf16[1,2048,1792]{2,1,0:T(8,128)(2,1)S(1)} %bitcast.11, ...), custom_call_target="tpu_custom_call" | custom-call | flops 5637144576 | bytes 1048576 | tf_op jit(solution)/shard_map/pallas_call | solution.py:43
  119.3 8.7 %shard_map.197 = (bf16[128,2048]{1,0:T(8,128)(2,1)S(1)}, bf16[128,2048]{1,0:T(8,128)(2,1)S(1)}) custom-call(bf16[128,2048]{1,0:T(8,128)(2,1)S(1)} %constant_dynamic-update-slice_fusion.16.own, bf16[128,2048]{1,0:T(8,128)(2,1)S(1)} %collective-permute-done.36.other, bf16[1,2048,1792]{2,1,0:T(8,128)(2,1)S(1)} %bitcast.9, bf16[1,2048,1792]{2,1,0:T(8,128)(2,1)S(1)} %bitcast.11, ...), custom_call_target="tpu_custom_call" | custom-call | flops 5637144576 | bytes 1048576 | tf_op jit(solution)/shard_map/pallas_call | solution.py:43
  128.0 8.9 %shard_map.198 = (bf16[128,2048]{1,0:T(8,128)(2,1)S(1)}, bf16[128,2048]{1,0:T(8,128)(2,1)S(1)}) custom-call(bf16[128,2048]{1,0:T(8,128)(2,1)S(1)} %constant_dynamic-update-slice_fusion.12.own, bf16[128,2048]{1,0:T(8,128)(2,1)S(1)} %collective-permute-done.31.other, bf16[1,2048,1792]{2,1,0:T(8,128)(2,1)S(1)} %bitcast.9, bf16[1,2048,1792]{2,1,0:T(8,128)(2,1)S(1)} %bitcast.11, ...), custom_call_target="tpu_custom_call" | custom-call | flops 5637144576 | bytes 1048576 | tf_op jit(solution)/shard_map/pallas_call | solution.py:43
  137.6 4.4 %collective-permute-start.15 = (bf16[32,2048]{1,0:T(8,128)(2,1)S(1)}, bf16[32,2048]{1,0:T(8,128)(2,1)S(1)}, u32[]{:S(2)}, u32[]{:S(2)}) collective-permute-start(bf16[32,2048]{1,0:T(8,128)(2,1)S(1)} %get-tuple-element.90), channel_id=1, source_target_pairs={{0,18},{2,16},{4,22},{6,20},{8,26},{10,24},{12,30},{14,28},{16,2},... | collective-permute-start | bytes 393224 | tf_op jit(solution)/shard_map/ppermute | solution.py:336
  142.2 7.7 %collective-permute-done.14.refs_0_ = bf16[32,2048]{1,0:T(8,128)(2,1)S(1)} collective-permute-done((bf16[32,2048]{1,0:T(8,128)(2,1)S(1)}, bf16[32,2048]{1,0:T(8,128)(2,1)S(1)}, u32[]{:S(2)}, u32[]{:S(2)}) %collective-permute-start.14) | collective-permute-done | bytes 131104 | tf_op jit(solution)/shard_map/ppermute | solution.py:336
  149.9 2.8 %collective-permute-done.15.refs_1_ = bf16[32,2048]{1,0:T(8,128)(2,1)S(1)} collective-permute-done((bf16[32,2048]{1,0:T(8,128)(2,1)S(1)}, bf16[32,2048]{1,0:T(8,128)(2,1)S(1)}, u32[]{:S(2)}, u32[]{:S(2)}) %collective-permute-start.15) | collective-permute-done | bytes 131104 | tf_op jit(solution)/shard_map/ppermute | solution.py:336
  152.7 3.6 %collective-permute-start.24 = (bf16[32,2048]{1,0:T(8,128)(2,1)S(1)}, bf16[32,2048]{1,0:T(8,128)(2,1)S(1)}, u32[]{:S(2)}, u32[]{:S(2)}) collective-permute-start(bf16[32,2048]{1,0:T(8,128)(2,1)S(1)} %get-tuple-element.101), channel_id=1, source_target_pairs={{0,8},{2,10},{4,12},{6,14},{8,0},{10,2},{12,4},{14,6},{16,24},{18,... | collective-permute-start | bytes 393224 | tf_op jit(solution)/shard_map/ppermute | solution.py:336
  156.3 3.1 %collective-permute-start.25 = (bf16[32,2048]{1,0:T(8,128)(2,1)S(1)}, bf16[32,2048]{1,0:T(8,128)(2,1)S(1)}, u32[]{:S(2)}, u32[]{:S(2)}) collective-permute-start(bf16[32,2048]{1,0:T(8,128)(2,1)S(1)} %get-tuple-element.102), channel_id=1, source_target_pairs={{0,10},{2,8},{4,14},{6,12},{8,2},{10,0},{12,6},{14,4},{16,26},{18,... | collective-permute-start | bytes 393224 | tf_op jit(solution)/shard_map/ppermute | solution.py:336
  159.8 4.2 %collective-permute-done.17.refs_3_ = bf16[32,2048]{1,0:T(8,128)(2,1)S(1)} collective-permute-done((bf16[32,2048]{1,0:T(8,128)(2,1)S(1)}, bf16[32,2048]{1,0:T(8,128)(2,1)S(1)}, u32[]{:S(2)}, u32[]{:S(2)}) %collective-permute-start.17) | collective-permute-done | bytes 131104 | tf_op jit(solution)/shard_map/ppermute | solution.py:336
  166.3 2.8 %collective-permute-start.40 = (bf16[32,2048]{1,0:T(8,128)(2,1)S(1)}, bf16[32,2048]{1,0:T(8,128)(2,1)S(1)}, u32[]{:S(2)}, u32[]{:S(2)}) collective-permute-start(bf16[32,2048]{1,0:T(8,128)(2,1)S(1)} %get-tuple-element.123), channel_id=1, source_target_pairs={{0,6},{2,4},{4,2},{6,0},{8,14},{10,12},{12,10},{14,8},{16,22},{18,... | collective-permute-start | bytes 393224 | tf_op jit(solution)/shard_map/ppermute | solution.py:336
  169.3 3.0 %collective-permute-start.42 = (bf16[32,2048]{1,0:T(8,128)(2,1)S(1)}, bf16[32,2048]{1,0:T(8,128)(2,1)S(1)}, u32[]{:S(2)}, u32[]{:S(2)}) collective-permute-start(bf16[32,2048]{1,0:T(8,128)(2,1)S(1)} %get-tuple-element.125), channel_id=1, source_target_pairs={{0,20},{2,22},{4,16},{6,18},{8,28},{10,30},{12,24},{14,26},{16,4},... | collective-permute-start | bytes 393224 | tf_op jit(solution)/shard_map/ppermute | solution.py:336
  172.3 2.6 %collective-permute-start.43 = (bf16[32,2048]{1,0:T(8,128)(2,1)S(1)}, bf16[32,2048]{1,0:T(8,128)(2,1)S(1)}, u32[]{:S(2)}, u32[]{:S(2)}) collective-permute-start(bf16[32,2048]{1,0:T(8,128)(2,1)S(1)} %get-tuple-element.126), channel_id=1, source_target_pairs={{0,22},{2,20},{4,18},{6,16},{8,30},{10,28},{12,26},{14,24},{16,6},... | collective-permute-start | bytes 393224 | tf_op jit(solution)/shard_map/ppermute | solution.py:336
  175.4 5.2 %collective-permute-done.39.refs_10_ = bf16[32,2048]{1,0:T(8,128)(2,1)S(1)} collective-permute-done((bf16[32,2048]{1,0:T(8,128)(2,1)S(1)}, bf16[32,2048]{1,0:T(8,128)(2,1)S(1)}, u32[]{:S(2)}, u32[]{:S(2)}) %collective-permute-start.39) | collective-permute-done | bytes 131104 | tf_op jit(solution)/shard_map/ppermute | solution.py:336
  180.6 3.0 %collective-permute-start.45 = (bf16[32,2048]{1,0:T(8,128)(2,1)S(1)}, bf16[32,2048]{1,0:T(8,128)(2,1)S(1)}, u32[]{:S(2)}, u32[]{:S(2)}) collective-permute-start(bf16[32,2048]{1,0:T(8,128)(2,1)S(1)} %get-tuple-element.128), channel_id=1, source_target_pairs={{0,30},{2,28},{4,26},{6,24},{8,22},{10,20},{12,18},{14,16},{16,14}... | collective-permute-start | bytes 393224 | tf_op jit(solution)/shard_map/ppermute | solution.py:336
  184.7 2.8 %collective-permute-done.43.refs_1_ = bf16[32,2048]{1,0:T(8,128)(2,1)S(1)} collective-permute-done((bf16[32,2048]{1,0:T(8,128)(2,1)S(1)}, bf16[32,2048]{1,0:T(8,128)(2,1)S(1)}, u32[]{:S(2)}, u32[]{:S(2)}) %collective-permute-start.43) | collective-permute-done | bytes 131104 | tf_op jit(solution)/shard_map/ppermute | solution.py:336
  187.5 4.4 %collective-permute-done.44.refs_2_ = bf16[32,2048]{1,0:T(8,128)(2,1)S(1)} collective-permute-done((bf16[32,2048]{1,0:T(8,128)(2,1)S(1)}, bf16[32,2048]{1,0:T(8,128)(2,1)S(1)}, u32[]{:S(2)}, u32[]{:S(2)}) %collective-permute-start.44) | collective-permute-done | bytes 131104 | tf_op jit(solution)/shard_map/ppermute | solution.py:336
  191.9 2.8 %collective-permute-done.45.refs_3_ = bf16[32,2048]{1,0:T(8,128)(2,1)S(1)} collective-permute-done((bf16[32,2048]{1,0:T(8,128)(2,1)S(1)}, bf16[32,2048]{1,0:T(8,128)(2,1)S(1)}, u32[]{:S(2)}, u32[]{:S(2)}) %collective-permute-start.45) | collective-permute-done | bytes 131104 | tf_op jit(solution)/shard_map/ppermute | solution.py:336
  (110 shorter events, 34.6 us)
Async XLA Ops:
  0.0 16.0 %collective-permute-start.7 = (bf16[512,2048]{1,0:T(8,128)(2,1)}, bf16[512,2048]{1,0:T(8,128)(2,1)S(1)}, u32[]{:S(2)}, u32[]{:S(2)}) collective-permute-start(bf16[512,2048]{1,0:T(8,128)(2,1)} %refs_6_.1), channel_id=1, source_target_pairs={{0,1},{1,0},{2,3},{3,2},{4,5},{5,4},{6,7},{7,6},{8,9},{9,8},{10,11... | collective-permute-start | bytes 6291464 | tf_op jit(solution)/shard_map/ppermute | solution.py:331
  28.4 41.4 %collective-permute-start.8 = (bf16[32,2048]{1,0:T(8,128)(2,1)S(1)}, bf16[32,2048]{1,0:T(8,128)(2,1)S(1)}, u32[]{:S(2)}, u32[]{:S(2)}) collective-permute-start(bf16[32,2048]{1,0:T(8,128)(2,1)S(1)} %get-tuple-element.80), channel_id=1, source_target_pairs={{0,16},{2,18},{4,20},{6,22},{8,24},{10,26},{12,28},{14,30},{16,0},... | collective-permute-start | bytes 393224 | tf_op jit(solution)/shard_map/ppermute | solution.py:336
  30.6 45.5 %collective-permute-start.9 = (bf16[32,2048]{1,0:T(8,128)(2,1)S(1)}, bf16[32,2048]{1,0:T(8,128)(2,1)S(1)}, u32[]{:S(2)}, u32[]{:S(2)}) collective-permute-start(bf16[32,2048]{1,0:T(8,128)(2,1)S(1)} %get-tuple-element.81), channel_id=1, source_target_pairs={{0,18},{2,16},{4,22},{6,20},{8,26},{10,24},{12,30},{14,28},{16,2},... | collective-permute-start | bytes 393224 | tf_op jit(solution)/shard_map/ppermute | solution.py:336
  33.0 45.8 %collective-permute-start.10 = (bf16[32,2048]{1,0:T(8,128)(2,1)S(1)}, bf16[32,2048]{1,0:T(8,128)(2,1)S(1)}, u32[]{:S(2)}, u32[]{:S(2)}) collective-permute-start(bf16[32,2048]{1,0:T(8,128)(2,1)S(1)} %get-tuple-element.82), channel_id=1, source_target_pairs={{0,24},{2,26},{4,28},{6,30},{8,16},{10,18},{12,20},{14,22},{16,8},... | collective-permute-start | bytes 393224 | tf_op jit(solution)/shard_map/ppermute | solution.py:336
  33.1 56.1 %collective-permute-start.11 = (bf16[32,2048]{1,0:T(8,128)(2,1)S(1)}, bf16[32,2048]{1,0:T(8,128)(2,1)S(1)}, u32[]{:S(2)}, u32[]{:S(2)}) collective-permute-start(bf16[32,2048]{1,0:T(8,128)(2,1)S(1)} %get-tuple-element.83), channel_id=1, source_target_pairs={{0,26},{2,24},{4,30},{6,28},{8,18},{10,16},{12,22},{14,20},{16,10}... | collective-permute-start | bytes 393224 | tf_op jit(solution)/shard_map/ppermute | solution.py:336
  34.9 22.7 %collective-permute-start.32 = (bf16[32,2048]{1,0:T(8,128)(2,1)S(1)}, bf16[32,2048]{1,0:T(8,128)(2,1)S(1)}, u32[]{:S(2)}, u32[]{:S(2)}) collective-permute-start(bf16[32,2048]{1,0:T(8,128)(2,1)S(1)} %get-tuple-element.109), channel_id=1, source_target_pairs={{0,20},{2,22},{4,16},{6,18},{8,28},{10,30},{12,24},{14,26},{16,4},... | collective-permute-start | bytes 393224 | tf_op jit(solution)/shard_map/ppermute | solution.py:336
  73.9 15.4 %collective-permute-start.21 = (bf16[32,2048]{1,0:T(8,128)(2,1)S(1)}, bf16[32,2048]{1,0:T(8,128)(2,1)S(1)}, u32[]{:S(2)}, u32[]{:S(2)}) collective-permute-start(bf16[32,2048]{1,0:T(8,128)(2,1)S(1)} %get-tuple-element.96), channel_id=1, source_target_pairs={{0,14},{2,12},{4,10},{6,8},{8,6},{10,4},{12,2},{14,0},{16,30},{18,... | collective-permute-start | bytes 393224 | tf_op jit(solution)/shard_map/ppermute | solution.py:336
  78.8 9.5 %collective-permute-start.30 = (bf16[32,2048]{1,0:T(8,128)(2,1)S(1)}, bf16[32,2048]{1,0:T(8,128)(2,1)S(1)}, u32[]{:S(2)}, u32[]{:S(2)}) collective-permute-start(bf16[32,2048]{1,0:T(8,128)(2,1)S(1)} %get-tuple-element.108), channel_id=1, source_target_pairs={{0,6},{2,4},{4,2},{6,0},{8,14},{10,12},{12,10},{14,8},{16,22},{18,... | collective-permute-start | bytes 393224 | tf_op jit(solution)/shard_map/ppermute | solution.py:336
  82.4 12.3 %collective-permute-start.33 = (bf16[32,2048]{1,0:T(8,128)(2,1)S(1)}, bf16[32,2048]{1,0:T(8,128)(2,1)S(1)}, u32[]{:S(2)}, u32[]{:S(2)}) collective-permute-start(bf16[32,2048]{1,0:T(8,128)(2,1)S(1)} %get-tuple-element.110), channel_id=1, source_target_pairs={{0,22},{2,20},{4,18},{6,16},{8,30},{10,28},{12,26},{14,24},{16,6},... | collective-permute-start | bytes 393224 | tf_op jit(solution)/shard_map/ppermute | solution.py:336
  85.3 13.9 %collective-permute-start.34 = (bf16[32,2048]{1,0:T(8,128)(2,1)S(1)}, bf16[32,2048]{1,0:T(8,128)(2,1)S(1)}, u32[]{:S(2)}, u32[]{:S(2)}) collective-permute-start(bf16[32,2048]{1,0:T(8,128)(2,1)S(1)} %get-tuple-element.111), channel_id=1, source_target_pairs={{0,28},{2,30},{4,24},{6,26},{8,20},{10,22},{12,16},{14,18},{16,12}... | collective-permute-start | bytes 393224 | tf_op jit(solution)/shard_map/ppermute | solution.py:336
  88.4 12.5 %collective-permute-start.35 = (bf16[32,2048]{1,0:T(8,128)(2,1)S(1)}, bf16[32,2048]{1,0:T(8,128)(2,1)S(1)}, u32[]{:S(2)}, u32[]{:S(2)}) collective-permute-start(bf16[32,2048]{1,0:T(8,128)(2,1)S(1)} %get-tuple-element.112), channel_id=1, source_target_pairs={{0,30},{2,28},{4,26},{6,24},{8,22},{10,20},{12,18},{14,16},{16,14}... | collective-permute-start | bytes 393224 | tf_op jit(solution)/shard_map/ppermute | solution.py:336
  89.2 38.8 %collective-permute-start.31 = (bf16[128,2048]{1,0:T(8,128)(2,1)S(1)}, bf16[128,2048]{1,0:T(8,128)(2,1)S(1)}, u32[]{:S(2)}, u32[]{:S(2)}) collective-permute-start(bf16[128,2048]{1,0:T(8,128)(2,1)S(1)} %constant_dynamic-update-slice_fusion.12.own), channel_id=1, source_target_pairs={{0,1},{1,0},{2,3},{3,2},{4,5},{5,4},{6,7},{7,6},{8,9},{9,8},{10,11... | collective-permute-start | bytes 1572872 | tf_op jit(solution)/shard_map/ppermute | solution.py:331
  89.3 11.6 %collective-permute-start.12 = (bf16[128,2048]{1,0:T(8,128)(2,1)S(1)}, bf16[128,2048]{1,0:T(8,128)(2,1)S(1)}, u32[]{:S(2)}, u32[]{:S(2)}) collective-permute-start(bf16[128,2048]{1,0:T(8,128)(2,1)S(1)} %constant_dynamic-update-slice_fusion.4.own), channel_id=1, source_target_pairs={{0,1},{1,0},{2,3},{3,2},{4,5},{5,4},{6,7},{7,6},{8,9},{9,8},{10,11... | collective-permute-start | bytes 1572872 | tf_op jit(solution)/shard_map/ppermute | solution.py:331
  94.7 15.6 %collective-permute-start.22 = (bf16[128,2048]{1,0:T(8,128)(2,1)S(1)}, bf16[128,2048]{1,0:T(8,128)(2,1)S(1)}, u32[]{:S(2)}, u32[]{:S(2)}) collective-permute-start(bf16[128,2048]{1,0:T(8,128)(2,1)S(1)} %constant_dynamic-update-slice_fusion.8.own), channel_id=1, source_target_pairs={{0,1},{1,0},{2,3},{3,2},{4,5},{5,4},{6,7},{7,6},{8,9},{9,8},{10,11... | collective-permute-start | bytes 1572872 | tf_op jit(solution)/shard_map/ppermute | solution.py:331
  100.8 18.4 %collective-permute-start.36 = (bf16[128,2048]{1,0:T(8,128)(2,1)S(1)}, bf16[128,2048]{1,0:T(8,128)(2,1)S(1)}, u32[]{:S(2)}, u32[]{:S(2)}) collective-permute-start(bf16[128,2048]{1,0:T(8,128)(2,1)S(1)} %constant_dynamic-update-slice_fusion.16.own), channel_id=1, source_target_pairs={{0,1},{1,0},{2,3},{3,2},{4,5},{5,4},{6,7},{7,6},{8,9},{9,8},{10,11... | collective-permute-start | bytes 1572872 | tf_op jit(solution)/shard_map/ppermute | solution.py:331
  119.0 23.0 %collective-permute-start.23 = (bf16[128,2048]{1,0:T(8,128)(2,1)S(1)}, bf16[128,2048]{1,0:T(8,128)(2,1)S(1)}, u32[]{:S(2)}, u32[]{:S(2)}) collective-permute-start(bf16[128,2048]{1,0:T(8,128)(2,1)S(1)} %get-tuple-element.100), channel_id=1, source_target_pairs={{0,1},{1,0},{2,3},{3,2},{4,5},{5,4},{6,7},{7,6},{8,9},{9,8},{10,11... | collective-permute-start | bytes 1572872 | tf_op jit(solution)/shard_map/ppermute | solution.py:331
  136.9 19.3 %collective-permute-start.37 = (bf16[128,2048]{1,0:T(8,128)(2,1)S(1)}, bf16[128,2048]{1,0:T(8,128)(2,1)S(1)}, u32[]{:S(2)}, u32[]{:S(2)}) collective-permute-start(bf16[128,2048]{1,0:T(8,128)(2,1)S(1)} %get-tuple-element.119), channel_id=1, source_target_pairs={{0,1},{1,0},{2,3},{3,2},{4,5},{5,4},{6,7},{7,6},{8,9},{9,8},{10,11... | collective-permute-start | bytes 1572872 | tf_op jit(solution)/shard_map/ppermute | solution.py:331
  137.5 28.8 %collective-permute-start.41 = (bf16[128,2048]{1,0:T(8,128)(2,1)S(1)}, bf16[128,2048]{1,0:T(8,128)(2,1)S(1)}, u32[]{:S(2)}, u32[]{:S(2)}) collective-permute-start(bf16[128,2048]{1,0:T(8,128)(2,1)S(1)} %get-tuple-element.124), channel_id=1, source_target_pairs={{0,1},{1,0},{2,3},{3,2},{4,5},{5,4},{6,7},{7,6},{8,9},{9,8},{10,11... | collective-permute-start | bytes 1572872 | tf_op jit(solution)/shard_map/ppermute | solution.py:331
  137.6 12.3 %collective-permute-start.14 = (bf16[32,2048]{1,0:T(8,128)(2,1)S(1)}, bf16[32,2048]{1,0:T(8,128)(2,1)S(1)}, u32[]{:S(2)}, u32[]{:S(2)}) collective-permute-start(bf16[32,2048]{1,0:T(8,128)(2,1)S(1)} %get-tuple-element.89), channel_id=1, source_target_pairs={{0,16},{2,18},{4,20},{6,22},{8,24},{10,26},{12,28},{14,30},{16,0},... | collective-permute-start | bytes 393224 | tf_op jit(solution)/shard_map/ppermute | solution.py:336
  137.6 15.1 %collective-permute-start.15 = (bf16[32,2048]{1,0:T(8,128)(2,1)S(1)}, bf16[32,2048]{1,0:T(8,128)(2,1)S(1)}, u32[]{:S(2)}, u32[]{:S(2)}) collective-permute-start(bf16[32,2048]{1,0:T(8,128)(2,1)S(1)} %get-tuple-element.90), channel_id=1, source_target_pairs={{0,18},{2,16},{4,22},{6,20},{8,26},{10,24},{12,30},{14,28},{16,2},... | collective-permute-start | bytes 393224 | tf_op jit(solution)/shard_map/ppermute | solution.py:336
  142.0 17.7 %collective-permute-start.16 = (bf16[32,2048]{1,0:T(8,128)(2,1)S(1)}, bf16[32,2048]{1,0:T(8,128)(2,1)S(1)}, u32[]{:S(2)}, u32[]{:S(2)}) collective-permute-start(bf16[32,2048]{1,0:T(8,128)(2,1)S(1)} %get-tuple-element.91), channel_id=1, source_target_pairs={{0,24},{2,26},{4,28},{6,30},{8,16},{10,18},{12,20},{14,22},{16,8},... | collective-permute-start | bytes 393224 | tf_op jit(solution)/shard_map/ppermute | solution.py:336
  149.9 14.1 %collective-permute-start.17 = (bf16[32,2048]{1,0:T(8,128)(2,1)S(1)}, bf16[32,2048]{1,0:T(8,128)(2,1)S(1)}, u32[]{:S(2)}, u32[]{:S(2)}) collective-permute-start(bf16[32,2048]{1,0:T(8,128)(2,1)S(1)} %get-tuple-element.92), channel_id=1, source_target_pairs={{0,26},{2,24},{4,30},{6,28},{8,18},{10,16},{12,22},{14,20},{16,10}... | collective-permute-start | bytes 393224 | tf_op jit(solution)/shard_map/ppermute | solution.py:336
  152.7 11.3 %collective-permute-start.24 = (bf16[32,2048]{1,0:T(8,128)(2,1)S(1)}, bf16[32,2048]{1,0:T(8,128)(2,1)S(1)}, u32[]{:S(2)}, u32[]{:S(2)}) collective-permute-start(bf16[32,2048]{1,0:T(8,128)(2,1)S(1)} %get-tuple-element.101), channel_id=1, source_target_pairs={{0,8},{2,10},{4,12},{6,14},{8,0},{10,2},{12,4},{14,6},{16,24},{18,... | collective-permute-start | bytes 393224 | tf_op jit(solution)/shard_map/ppermute | solution.py:336
  156.3 9.4 %collective-permute-start.25 = (bf16[32,2048]{1,0:T(8,128)(2,1)S(1)}, bf16[32,2048]{1,0:T(8,128)(2,1)S(1)}, u32[]{:S(2)}, u32[]{:S(2)}) collective-permute-start(bf16[32,2048]{1,0:T(8,128)(2,1)S(1)} %get-tuple-element.102), channel_id=1, source_target_pairs={{0,10},{2,8},{4,14},{6,12},{8,2},{10,0},{12,6},{14,4},{16,26},{18,... | collective-permute-start | bytes 393224 | tf_op jit(solution)/shard_map/ppermute | solution.py:336
  159.8 9.5 %collective-permute-start.26 = (bf16[32,2048]{1,0:T(8,128)(2,1)S(1)}, bf16[32,2048]{1,0:T(8,128)(2,1)S(1)}, u32[]{:S(2)}, u32[]{:S(2)}) collective-permute-start(bf16[32,2048]{1,0:T(8,128)(2,1)S(1)} %get-tuple-element.103), channel_id=1, source_target_pairs={{0,12},{2,14},{4,8},{6,10},{8,4},{10,6},{12,0},{14,2},{16,28},{18,... | collective-permute-start | bytes 393224 | tf_op jit(solution)/shard_map/ppermute | solution.py:336
  164.0 10.8 %collective-permute-start.38 = (bf16[32,2048]{1,0:T(8,128)(2,1)S(1)}, bf16[32,2048]{1,0:T(8,128)(2,1)S(1)}, u32[]{:S(2)}, u32[]{:S(2)}) collective-permute-start(bf16[32,2048]{1,0:T(8,128)(2,1)S(1)} %get-tuple-element.121), channel_id=1, source_target_pairs={{0,2},{2,0},{4,6},{6,4},{8,10},{10,8},{12,14},{14,12},{16,18},{18,... | collective-permute-start | bytes 393224 | tf_op jit(solution)/shard_map/ppermute | solution.py:336
  165.7 14.9 %collective-permute-start.39 = (bf16[32,2048]{1,0:T(8,128)(2,1)S(1)}, bf16[32,2048]{1,0:T(8,128)(2,1)S(1)}, u32[]{:S(2)}, u32[]{:S(2)}) collective-permute-start(bf16[32,2048]{1,0:T(8,128)(2,1)S(1)} %get-tuple-element.122), channel_id=1, source_target_pairs={{0,4},{2,6},{4,0},{6,2},{8,12},{10,14},{12,8},{14,10},{16,20},{18,... | collective-permute-start | bytes 393224 | tf_op jit(solution)/shard_map/ppermute | solution.py:336
  166.3 17.2 %collective-permute-start.40 = (bf16[32,2048]{1,0:T(8,128)(2,1)S(1)}, bf16[32,2048]{1,0:T(8,128)(2,1)S(1)}, u32[]{:S(2)}, u32[]{:S(2)}) collective-permute-start(bf16[32,2048]{1,0:T(8,128)(2,1)S(1)} %get-tuple-element.123), channel_id=1, source_target_pairs={{0,6},{2,4},{4,2},{6,0},{8,14},{10,12},{12,10},{14,8},{16,22},{18,... | collective-permute-start | bytes 393224 | tf_op jit(solution)/shard_map/ppermute | solution.py:336
  169.3 15.4 %collective-permute-start.42 = (bf16[32,2048]{1,0:T(8,128)(2,1)S(1)}, bf16[32,2048]{1,0:T(8,128)(2,1)S(1)}, u32[]{:S(2)}, u32[]{:S(2)}) collective-permute-start(bf16[32,2048]{1,0:T(8,128)(2,1)S(1)} %get-tuple-element.125), channel_id=1, source_target_pairs={{0,20},{2,22},{4,16},{6,18},{8,28},{10,30},{12,24},{14,26},{16,4},... | collective-permute-start | bytes 393224 | tf_op jit(solution)/shard_map/ppermute | solution.py:336
  172.3 15.2 %collective-permute-start.43 = (bf16[32,2048]{1,0:T(8,128)(2,1)S(1)}, bf16[32,2048]{1,0:T(8,128)(2,1)S(1)}, u32[]{:S(2)}, u32[]{:S(2)}) collective-permute-start(bf16[32,2048]{1,0:T(8,128)(2,1)S(1)} %get-tuple-element.126), channel_id=1, source_target_pairs={{0,22},{2,20},{4,18},{6,16},{8,30},{10,28},{12,26},{14,24},{16,6},... | collective-permute-start | bytes 393224 | tf_op jit(solution)/shard_map/ppermute | solution.py:336
  174.8 17.1 %collective-permute-start.44 = (bf16[32,2048]{1,0:T(8,128)(2,1)S(1)}, bf16[32,2048]{1,0:T(8,128)(2,1)S(1)}, u32[]{:S(2)}, u32[]{:S(2)}) collective-permute-start(bf16[32,2048]{1,0:T(8,128)(2,1)S(1)} %get-tuple-element.127), channel_id=1, source_target_pairs={{0,28},{2,30},{4,24},{6,26},{8,20},{10,22},{12,16},{14,18},{16,12}... | collective-permute-start | bytes 393224 | tf_op jit(solution)/shard_map/ppermute | solution.py:336
  180.6 14.2 %collective-permute-start.45 = (bf16[32,2048]{1,0:T(8,128)(2,1)S(1)}, bf16[32,2048]{1,0:T(8,128)(2,1)S(1)}, u32[]{:S(2)}, u32[]{:S(2)}) collective-permute-start(bf16[32,2048]{1,0:T(8,128)(2,1)S(1)} %get-tuple-element.128), channel_id=1, source_target_pairs={{0,30},{2,28},{4,26},{6,24},{8,22},{10,20},{12,18},{14,16},{16,14}... | collective-permute-start | bytes 393224 | tf_op jit(solution)/shard_map/ppermute | solution.py:336
  (20 other events, 560.9 us)

commit v2 on v1

--- a/solution.py
+++ b/solution.py
@@ -33,15 +33,22 @@
     return lax.broadcasted_iota(jnp.int32, shape, axis)
 
 
-def call(body, outs, args, flops, limit=12, scalars=0, hbm=(), scratch=()):
+def call(body, outs, args, flops, limit=12, scalars=0, hbm=(), scratch=(), after=()):
     specs = [
         pl.BlockSpec(memory_space=pltpu.SMEM)
         if k < scalars
         else pl.BlockSpec(memory_space=pl.ANY if k in hbm else pltpu.VMEM)
         for k in range(len(args))
     ]
+    count = len(args)
+    args = [*args, *after]
+    specs += [pl.BlockSpec(memory_space=pl.ANY)] * len(after)
+
+    def ordered(*refs):
+        body(*refs[:count], *refs[len(args) :])
+
     return pl.pallas_call(
-        body,
+        ordered,
         out_shape=outs,
         in_specs=specs,
         out_specs=jax.tree.map(lambda _: pl.BlockSpec(memory_space=pltpu.VMEM), outs),
@@ -96,7 +103,9 @@
     send[...] = own[part, :]
 
 
-def ready_kernel(where, content, content_far, turning, turning_far, docs, routes, nc, ns, bc, bs, queries, pick0, pick1, *, capacity):
+def ready_kernel(where, content, content_far, turning, turning_far, docs, routes, nc, ns, bc, bs, down, queries, pick0, pick1, down_held, sem, *, capacity):
+    copy = pltpu.make_async_copy(down, down_held, sem)
+    copy.start()
     sp, tp = where[0], where[1]
     rows = content.shape[0]
     heads_here = HEADS // 2
@@ -132,6 +141,7 @@
     for route, pick in ((first, pick0), (second, pick1)):
         place = jnp.sum(jnp.where(route == lane, rank, 0.0), 1, keepdims=True).astype(jnp.int32)
         pick[...] = (slot == (route ^ sp) * capacity + place).astype(BF16)
+    copy.wait()
 
 
 def layer_norm(values, gain):
@@ -143,17 +153,18 @@
 
 def attend_kernel(where, *refs, near, pieces, capacity):
     kv_own, kv_near = refs[0], refs[1 : 1 + near]
-    queries, key_up, value_up, out_mine, out_theirs, residual, gain, pick0, pick1, down = refs[
-        1 + near : 11 + near
+    queries, key_up, value_up, out_mine, out_theirs, residual, gain, pick0, pick1, gate, up = refs[
+        1 + near : 12 + near
     ]
-    normed, down_held = refs[11 + near : 13 + near]
-    outbound = refs[13 + near : 13 + near + pieces]
-    packed, keys, values, attended, summed, w_mine, w_theirs, sems = refs[13 + near + pieces :]
+    normed, gate_held, up_held = refs[12 + near : 15 + near]
+    outbound = refs[15 + near : 15 + near + pieces]
+    packed, keys, values, attended, summed, w_mine, w_theirs, sems = refs[15 + near + pieces :]
     tp = where[1]
     copies = [
         pltpu.make_async_copy(out_mine, w_mine, sems.at[0]),
         pltpu.make_async_copy(out_theirs, w_theirs, sems.at[1]),
-        pltpu.make_async_copy(down, down_held, sems.at[2]),
+        pltpu.make_async_copy(gate, gate_held, sems.at[2]),
+        pltpu.make_async_copy(up, up_held, sems.at[3]),
     ]
     for copy in copies:
         copy.start()
@@ -187,7 +198,7 @@
         attended[:, pl.ds(pl.multiple_of(head * DV, LANES), DV)] = mixed.astype(BF16)
         return carry
 
-    lax.fori_loop(0, HEADS, head_step, 0)
+    lax.fori_loop(0, HEADS, head_step, 0, unroll=True)
     half = w_mine.shape[0]
     copies[0].wait()
     summed[...] = dot(attended[:, :half], w_mine[...]).astype(BF16).astype(F32)
@@ -207,45 +218,36 @@
     for k, ref in enumerate(outbound):
         ref[...] = placed[k * capacity : (k + 1) * capacity]
     copies[2].wait()
-
-
-def expert_kernel(own, other, w_gate, w_up, w_down, mine, theirs, rows_in, hidden, *, tile):
+    copies[3].wait()
+
+
+def expert_kernel(own, other, w_gate, w_up, w_down, mine, theirs):
     half = own.shape[0]
-    rows_in[:half, :] = own[...]
-    rows_in[half:, :] = other[...]
-
-    def hidden_step(step, carry):
-        cols = pl.ds(pl.multiple_of(step * tile, tile), tile)
-        value = rows_in[...]
-        gate = dot(value, w_gate[0, :, cols])
-        upward = dot(value, w_up[0, :, cols])
-        hidden[:, cols] = (gate / (1.0 + jnp.exp(-gate)) * upward).astype(BF16)
-        return carry
-
-    lax.fori_loop(0, hidden.shape[1] // tile, hidden_step, 0)
-
-    def down_step(step, carry):
-        cols = pl.ds(pl.multiple_of(step * tile, tile), tile)
-        partial = dot(hidden[...], w_down[0, :, cols]).astype(BF16)
-        mine[:, cols] = partial[:half]
-        theirs[:, cols] = partial[half:]
-        return carry
-
-    lax.fori_loop(0, mine.shape[1] // tile, down_step, 0)
-
-
-def experts(own, other, w_gate, w_up, w_down):
+    value = jnp.concatenate([own[...], other[...]], 0)
+    gate = dot(value, w_gate[0])
+    upward = dot(value, w_up[0])
+    hidden = (gate / (1.0 + jnp.exp(-gate)) * upward).astype(BF16)
+    partial = dot(hidden, w_down[0]).astype(BF16)
+    mine[...] = partial[:half]
+    theirs[...] = partial[half:]
+
+
+def experts(own, other, w_gate, w_up, w_down, after):
     half, width = own.shape
     hidden = w_gate.shape[2]
     rows = 2 * half
     return call(
-        functools.partial(expert_kernel, tile=256),
+        expert_kernel,
         [shape(half, width)] * 2,
         [own, other, w_gate, w_up, w_down],
         6 * rows * width * hidden,
-        limit=14,
-        scratch=[pltpu.VMEM((rows, width), BF16), pltpu.VMEM((rows, hidden), BF16)],
-    )
+        limit=18,
+        after=after,
+    )
+
+
+def mark_kernel(value, out):
+    out[...] = value[...]
 
 
 def add_kernel(a, b, *outs):
@@ -356,26 +358,35 @@
         mine = lax.dynamic_slice_in_dim(value, tp * rows, rows, 0)
         return mine, across(lax.dynamic_slice_in_dim(value, (1 - tp) * rows, rows, 0))
 
-    queries_ready, pick0, pick1 = call(
+    args = [where, *split(queries_content), *split(queries_rotary), far(docs), far(routes.T)]
+    args += [*map(far, tables), far(w_down)]
+    queries_ready, pick0, pick1, w_down = call(
         functools.partial(ready_kernel, capacity=capacity),
-        [shape(rows, HEADS * 256), shape(rows, chips * capacity), shape(rows, chips * capacity)],
-        [where, *split(queries_content), *split(queries_rotary), far(docs), far(routes.T), *map(far, tables)],
+        [
+            shape(rows, HEADS * 256),
+            shape(rows, chips * capacity),
+            shape(rows, chips * capacity),
+            shape(*w_down.shape),
+        ],
+        args,
         1 << 26,
         scalars=1,
+        hbm=(len(args) - 1,),
+        scratch=[pltpu.SemaphoreType.DMA],
     )
     kv_near, queries_ready = lax.optimization_barrier((kv_near, queries_ready))
     kv_all = [jnp.concatenate(kv_near, 0)]
     kv_all.append(across(kv_all[0]))
     reach = tok_dev + sum(value.shape[0] for value in kv_all)
     args = [where, kv_own, *kv_all, queries_ready, far(w_key_up), far(w_value_up), far(w_out), out_theirs]
-    hbm = (len(args) - 2, len(args) - 1, len(args) + 4)
-    args += [far(residual), far(norm_gain.reshape(1, width)), pick0, pick1, far(w_down)]
-    normed, w_down, *outbound = call(
+    hbm = (len(args) - 2, len(args) - 1, len(args) + 4, len(args) + 5)
+    args += [far(residual), far(norm_gain.reshape(1, width)), pick0, pick1, far(w_gate), far(w_up)]
+    normed, w_gate, w_up, *outbound = call(
         functools.partial(attend_kernel, near=len(kv_all), pieces=chips, capacity=capacity),
-        [shape(rows, width), shape(*w_down.shape)] + [shape(capacity, width)] * chips,
+        [shape(rows, width), shape(*w_gate.shape), shape(*w_up.shape)] + [shape(capacity, width)] * chips,
         args,
         1 << 32,
-        limit=34,
+        limit=20,
         scalars=1,
         hbm=hbm,
         scratch=[
@@ -386,31 +397,54 @@
             pltpu.VMEM((rows, width), F32),
             pltpu.VMEM(w_out.shape, BF16),
             pltpu.VMEM(w_out.shape, BF16),
-            pltpu.SemaphoreType.DMA((3,)),
+            pltpu.SemaphoreType.DMA((4,)),
         ],
     )
     groups = group_order(chips)
     w_gate, w_up, w_down = (
         pltpu.with_memory_space_constraint(w, pltpu.VMEM) for w in (w_gate, w_up, w_down)
     )
-    landed, returned, done = {}, {}, {}
-    for number in (0, 2, 3, 1):
-        for s in groups[number]:
-            landed[s] = exchange(outbound[s], s)
-    after = ()
-    for number in (0, 2, 1, 3):
+    landed, returned = {}, {}
+
+    def send(number, pieces):
+        for s, piece in zip(groups[number], pieces):
+            landed[s] = exchange(piece, s)
+
+    halves = {}
+
+    def give_back(number, *after):
         group = groups[number]
-        own = jnp.concatenate([landed[s] for s in group], 0)
+        done = call(
+            add_kernel, [shape(capacity, width)] * len(group), halves[number], 1 << 20, after=after
+        )
+        for s, value in zip(group, done):
+            returned[s] = exchange(value, s)
+        return done
+
+    def mark(*after):
+        return call(mark_kernel, shape(8, LANES), [pick0[:8, :LANES]], 1 << 20, after=after)
+
+    def work(number, *after):
+        own = jnp.concatenate([landed[s] for s in groups[number]], 0)
         other = across(own)
-        own, other, _ = lax.optimization_barrier((own, other, after))
-        mine, theirs = experts(own, other, w_gate, w_up, w_down)
-        after = (mine, done.get(0, ()), done.get(1, ()))
-        done[number] = call(
-            add_kernel, [shape(capacity, width)] * len(group), [mine, across(theirs)], 1 << 20
-        )
-        for s, value in zip(group, done[number]):
-            returned[s] = exchange(value, s)
-    early, late = groups[0] + groups[2] + groups[3], groups[1]
+        return experts(own, other, w_gate, w_up, w_down, after)
+
+    far_a, far_b, next_plane, plane = range(4)
+    for number in (far_a, plane, next_plane, far_b):
+        send(number, [outbound[s] for s in groups[number]])
+    mine, theirs = work(plane, mark())
+    halves[plane] = (mine, across(theirs))
+    mine, theirs = work(far_a, mine)
+    halves[far_a] = (mine, across(theirs))
+    marked = mark(give_back(far_a)[0])
+    mine, theirs = work(next_plane, marked)
+    halves[next_plane] = (mine, across(theirs))
+    mine, theirs = work(far_b, mine)
+    halves[far_b] = (mine, across(theirs))
+    last = give_back(far_b)[0]
+    give_back(plane, last)
+    give_back(next_plane, last)
+    early, late = groups[far_a], groups[far_b] + groups[plane] + groups[next_plane]
 
     def gathered(total, pieces, body, out, extra=()):
         return call(

time: 197 us -> 166 us (0.84)
  waiting for transfers between devices: 74 us -> 53.6 us
  Pallas kernels: 53.9 us -> 43.3 us
    ppermute x30, waiting for transfers between devices: 69.5 us -> 46.3 us  [exchange(): return lax.ppermute(value, 'sp', [(j, j ^ s) for j in range(chips)])]
    pallas_call x13 -> x15, Pallas kernels: 53.9 us -> 43.3 us  [call(): pl.pallas_call(ordered, out_shape=outs, in_specs=specs, out_specs=jax.tre...]
  transfers between devices with their start and end apart: 46 -> 46, of which waited for: 22 -> 17; matrix products, arithmetic and copies ran while one was open for 1% -> 1% of each run, Pallas kernels for 20% -> 15%
where the time goes in v2:
time: 166 us
  starting transfers between devices  66.2 us (40%)
  waiting for transfers between devices  53.6 us (32%)
  Pallas kernels  43.3 us (26%)
  local copies, waits for them, and re-layouts  2.12 us (1%)
    ppermute x30, starting transfers between devices, exchange(): return lax.ppermute(value, 'sp', [(j, j ^ s) for j in range(chips)])  58.7 us
    ppermute x30, waiting for transfers between devices, exchange(): return lax.ppermute(value, 'sp', [(j, j ^ s) for j in range(chips)])  46.3 us
    pallas_call x15, Pallas kernels, call(): pl.pallas_call(ordered, out_shape=outs, in_specs=specs, out_specs=jax.tre...  43.3 us
    ppermute x4, starting transfers between devices, per_device(): lax.ppermute(kv_send, 'sp', [(j, (j + d) % chips) for j in range(chips)])  4.82 us
    ppermute x4, waiting for transfers between devices, per_device(): lax.ppermute(kv_send, 'sp', [(j, (j + d) % chips) for j in range(chips)])  4.36 us
  transfers between devices with their start and end apart: 46, of which 17 were waited for; matrix products, arithmetic and copies ran while one was open for 1% of the time, Pallas kernels for 15%

profile of v2, /device:TPU:16, one launch (start us, length us, event | category | flops | bytes accessed | tf_op | source)
XLA Modules:
  0.0 165.7 jit_solution(13900643542309447779)
XLA Ops:
  5.6 2.4 %collective-permute-start.1 = (bf16[128,384]{1,0:T(8,128)(2,1)S(1)}, bf16[128,384]{1,0:T(8,128)(2,1)S(1)}, u32[]{:S(2)}, u32[]{:S(2)}) collective-permute-start(bf16[128,384]{1,0:T(8,128)(2,1)S(1)} %get-tuple-element.62), channel_id=1, source_target_pairs={{0,6},{2,8},{4,10},{6,12},{8,14},{10,16},{12,18},{14,20},{16,22},{... | collective-permute-start | bytes 294920 | tf_op jit(solution)/shard_map/ppermute | solution.py:349
  8.8 4.2 %shard_map.191 = (bf16[128,2048]{1,0:T(8,128)(2,1)S(1)}, bf16[128,512]{1,0:T(8,128)(2,1)S(1)}, bf16[128,512]{1,0:T(8,128)(2,1)S(1)}, bf16[1,1792,2048]{2,1,0:T(8,128)(2,1)S(1)}) custom-call(s32[2]{0:T(128)S(1)} %pad_add_fusion.refs_0_, bf16[128,512]{1,0:T(8,128)(2,1)S(1)} %get-tuple-element.118.refs_1_, bf16[128,512]{1,0:T(8,128)(2,1)S(1)} %collective-permute-done.4.refs_2_, ...), custom_call_target="tpu_custom_call" | custom-call | flops 67108864 | bytes 1048576 | tf_op jit(solution)/shard_map/pallas_call | solution.py:50
  14.4 3.0 %collective-permute-done.3 = bf16[128,384]{1,0:T(8,128)(2,1)S(1)} collective-permute-done((bf16[128,384]{1,0:T(8,128)(2,1)S(1)}, bf16[128,384]{1,0:T(8,128)(2,1)S(1)}, u32[]{:S(2)}, u32[]{:S(2)}) %collective-permute-start.3) | collective-permute-done | bytes 98336 | tf_op jit(solution)/shard_map/ppermute | solution.py:349
  19.2 10.2 %shard_map.192 = (bf16[128,2048]{1,0:T(8,128)(2,1)S(1)}, bf16[1,2048,1792]{2,1,0:T(8,128)(2,1)S(1)}, bf16[1,2048,1792]{2,1,0:T(8,128)(2,1)S(1)}, bf16[32,2048]{1...) custom-call(s32[2]{0:T(128)S(1)} %pad_add_fusion.refs_0_, ...), custom_call_target="tpu_custom_call" | custom-call | flops 4294967296 | bytes 1048576 | tf_op jit(solution)/shard_map/pallas_call | solution.py:50
  29.7 3.3 %collective-permute-start.15 = (bf16[32,2048]{1,0:T(8,128)(2,1)S(1)}, bf16[32,2048]{1,0:T(8,128)(2,1)S(1)}, u32[]{:S(2)}, u32[]{:S(2)}) collective-permute-start(bf16[32,2048]{1,0:T(8,128)(2,1)S(1)} %get-tuple-element.84), channel_id=1, source_target_pairs={{0,6},{2,4},{4,2},{6,0},{8,14},{10,12},{12,10},{14,8},{16,22},{18,... | collective-permute-start | bytes 393224 | tf_op jit(solution)/shard_map/ppermute | solution.py:338
  33.0 2.3 %collective-permute-start.8 = (bf16[32,2048]{1,0:T(8,128)(2,1)S(1)}, bf16[32,2048]{1,0:T(8,128)(2,1)S(1)}, u32[]{:S(2)}, u32[]{:S(2)}) collective-permute-start(bf16[32,2048]{1,0:T(8,128)(2,1)S(1)} %get-tuple-element.74), channel_id=1, source_target_pairs={{0,16},{2,18},{4,20},{6,22},{8,24},{10,26},{12,28},{14,30},{16,0},... | collective-permute-start | bytes 393224 | tf_op jit(solution)/shard_map/ppermute | solution.py:338
  35.4 7.0 %collective-permute-done.8 = bf16[32,2048]{1,0:T(8,128)(2,1)S(1)} collective-permute-done((bf16[32,2048]{1,0:T(8,128)(2,1)S(1)}, bf16[32,2048]{1,0:T(8,128)(2,1)S(1)}, u32[]{:S(2)}, u32[]{:S(2)}) %collective-permute-start.8) | collective-permute-done | bytes 131104 | tf_op jit(solution)/shard_map/ppermute | solution.py:338
  42.4 3.5 %collective-permute-start.27 = (bf16[32,2048]{1,0:T(8,128)(2,1)S(1)}, bf16[32,2048]{1,0:T(8,128)(2,1)S(1)}, u32[]{:S(2)}, u32[]{:S(2)}) collective-permute-start(bf16[32,2048]{1,0:T(8,128)(2,1)S(1)} %get-tuple-element.96), channel_id=1, source_target_pairs={{0,8},{2,10},{4,12},{6,14},{8,0},{10,2},{12,4},{14,6},{16,24},{18,... | collective-permute-start | bytes 393224 | tf_op jit(solution)/shard_map/ppermute | solution.py:338
  45.9 3.2 %collective-permute-done.27 = bf16[32,2048]{1,0:T(8,128)(2,1)S(1)} collective-permute-done((bf16[32,2048]{1,0:T(8,128)(2,1)S(1)}, bf16[32,2048]{1,0:T(8,128)(2,1)S(1)}, u32[]{:S(2)}, u32[]{:S(2)}) %collective-permute-start.27) | collective-permute-done | bytes 131104 | tf_op jit(solution)/shard_map/ppermute | solution.py:338
  50.9 5.1 %collective-permute-done.22 = bf16[32,2048]{1,0:T(8,128)(2,1)S(1)} collective-permute-done((bf16[32,2048]{1,0:T(8,128)(2,1)S(1)}, bf16[32,2048]{1,0:T(8,128)(2,1)S(1)}, u32[]{:S(2)}, u32[]{:S(2)}) %collective-permute-start.22) | collective-permute-done | bytes 131104 | tf_op jit(solution)/shard_map/ppermute | solution.py:338
  58.0 6.5 %collective-permute-start.28 = (bf16[32,2048]{1,0:T(8,128)(2,1)S(1)}, bf16[32,2048]{1,0:T(8,128)(2,1)S(1)}, u32[]{:S(2)}, u32[]{:S(2)}) collective-permute-start(bf16[32,2048]{1,0:T(8,128)(2,1)S(1)} %get-tuple-element.97), channel_id=1, source_target_pairs={{0,10},{2,8},{4,14},{6,12},{8,2},{10,0},{12,6},{14,4},{16,26},{18,... | collective-permute-start | bytes 393224 | tf_op jit(solution)/shard_map/ppermute | solution.py:338
  64.6 3.3 %collective-permute-start.30 = (bf16[32,2048]{1,0:T(8,128)(2,1)S(1)}, bf16[32,2048]{1,0:T(8,128)(2,1)S(1)}, u32[]{:S(2)}, u32[]{:S(2)}) collective-permute-start(bf16[32,2048]{1,0:T(8,128)(2,1)S(1)} %get-tuple-element.99), channel_id=1, source_target_pairs={{0,14},{2,12},{4,10},{6,8},{8,6},{10,4},{12,2},{14,0},{16,30},{18,... | collective-permute-start | bytes 393224 | tf_op jit(solution)/shard_map/ppermute | solution.py:338
  69.8 3.6 %collective-permute-start.24 = (bf16[32,2048]{1,0:T(8,128)(2,1)S(1)}, bf16[32,2048]{1,0:T(8,128)(2,1)S(1)}, u32[]{:S(2)}, u32[]{:S(2)}) collective-permute-start(bf16[32,2048]{1,0:T(8,128)(2,1)S(1)} %get-tuple-element.94), channel_id=1, source_target_pairs={{0,28},{2,30},{4,24},{6,26},{8,20},{10,22},{12,16},{14,18},{16,12}... | collective-permute-start | bytes 393224 | tf_op jit(solution)/shard_map/ppermute | solution.py:338
  73.4 2.2 %collective-permute-done.29 = bf16[32,2048]{1,0:T(8,128)(2,1)S(1)} collective-permute-done((bf16[32,2048]{1,0:T(8,128)(2,1)S(1)}, bf16[32,2048]{1,0:T(8,128)(2,1)S(1)}, u32[]{:S(2)}, u32[]{:S(2)}) %collective-permute-start.29) | collective-permute-done | bytes 131104 | tf_op jit(solution)/shard_map/ppermute | solution.py:338
  77.5 2.1 %collective-permute-done.30 = bf16[32,2048]{1,0:T(8,128)(2,1)S(1)} collective-permute-done((bf16[32,2048]{1,0:T(8,128)(2,1)S(1)}, bf16[32,2048]{1,0:T(8,128)(2,1)S(1)}, u32[]{:S(2)}, u32[]{:S(2)}) %collective-permute-start.30) | collective-permute-done | bytes 131104 | tf_op jit(solution)/shard_map/ppermute | solution.py:338
  80.2 6.0 %shard_map.194 = (bf16[128,2048]{1,0:T(8,128)(2,1)S(1)}, bf16[128,2048]{1,0:T(8,128)(2,1)S(1)}) custom-call(bf16[128,2048]{1,0:T(8,128)(2,1)S(1)} %constant_dynamic-update-slice_fusion.8.refs_0_, bf16[128,2048]{1,0:T(8,128)(2,1)S(1)} %collective-permute-done.16.refs_1_, bf16[1,2048,1792]{2,1,0:T(8,128)(2,1)S(1)} %get-tuple-element.78.refs_2_, ...), custom_call_target="tpu_custom_call" | custom-call | flops 5637144576 | bytes 1048576 | tf_op jit(solution)/shard_map/pallas_call | solution.py:50
  86.2 6.0 %shard_map.195 = (bf16[128,2048]{1,0:T(8,128)(2,1)S(1)}, bf16[128,2048]{1,0:T(8,128)(2,1)S(1)}) custom-call(bf16[128,2048]{1,0:T(8,128)(2,1)S(1)} %constant_dynamic-update-slice_fusion.4.refs_0_, bf16[128,2048]{1,0:T(8,128)(2,1)S(1)} %collective-permute-done.12.refs_1_, bf16[1,2048,1792]{2,1,0:T(8,128)(2,1)S(1)} %get-tuple-element.78.refs_2_, ...), custom_call_target="tpu_custom_call" | custom-call | flops 5637144576 | bytes 1048576 | tf_op jit(solution)/shard_map/pallas_call | solution.py:50
  94.3 6.2 %shard_map.199 = (bf16[128,2048]{1,0:T(8,128)(2,1)S(1)}, bf16[128,2048]{1,0:T(8,128)(2,1)S(1)}) custom-call(bf16[128,2048]{1,0:T(8,128)(2,1)S(1)} %constant_dynamic-update-slice_fusion.16.refs_0_, bf16[128,2048]{1,0:T(8,128)(2,1)S(1)} %collective-permute-done.31.refs_1_, bf16[1,2048,1792]{2,1,0:T(8,128)(2,1)S(1)} %get-tuple-element.78.refs_2_, ...), custom_call_target="tpu_custom_call" | custom-call | flops 5637144576 | bytes 1048576 | tf_op jit(solution)/shard_map/pallas_call | solution.py:50
  100.5 6.0 %shard_map.200 = (bf16[128,2048]{1,0:T(8,128)(2,1)S(1)}, bf16[128,2048]{1,0:T(8,128)(2,1)S(1)}) custom-call(bf16[128,2048]{1,0:T(8,128)(2,1)S(1)} %constant_dynamic-update-slice_fusion.12.refs_0_, bf16[128,2048]{1,0:T(8,128)(2,1)S(1)} %collective-permute-done.26.refs_1_, bf16[1,2048,1792]{2,1,0:T(8,128)(2,1)S(1)} %get-tuple-element.78.refs_2_, ...), custom_call_target="tpu_custom_call" | custom-call | flops 5637144576 | bytes 1048576 | tf_op jit(solution)/shard_map/pallas_call | solution.py:50
  107.2 2.8 %collective-permute-start.18 = (bf16[32,2048]{1,0:T(8,128)(2,1)S(1)}, bf16[32,2048]{1,0:T(8,128)(2,1)S(1)}, u32[]{:S(2)}, u32[]{:S(2)}) collective-permute-start(bf16[32,2048]{1,0:T(8,128)(2,1)S(1)} %get-tuple-element.88.refs_1_), channel_id=1, source_target_pairs={{0,16},{2,18},{4,20},{6,22},{8,24},{10,26},{12,28},{14,30},{16,0},... | collective-permute-start | bytes 393224 | tf_op jit(solution)/shard_map/ppermute | solution.py:338
  113.4 3.9 %collective-permute-start.42 = (bf16[32,2048]{1,0:T(8,128)(2,1)S(1)}, bf16[32,2048]{1,0:T(8,128)(2,1)S(1)}, u32[]{:S(2)}, u32[]{:S(2)}) collective-permute-start(bf16[32,2048]{1,0:T(8,128)(2,1)S(1)} %get-tuple-element.113), channel_id=1, source_target_pairs={{0,8},{2,10},{4,12},{6,14},{8,0},{10,2},{12,4},{14,6},{16,24},{18,... | collective-permute-start | bytes 393224 | tf_op jit(solution)/shard_map/ppermute | solution.py:338
  117.5 6.8 %collective-permute-done.18.refs_4_ = bf16[32,2048]{1,0:T(8,128)(2,1)S(1)} collective-permute-done((bf16[32,2048]{1,0:T(8,128)(2,1)S(1)}, bf16[32,2048]{1,0:T(8,128)(2,1)S(1)}, u32[]{:S(2)}, u32[]{:S(2)}) %collective-permute-start.18) | collective-permute-done | bytes 131104 | tf_op jit(solution)/shard_map/ppermute | solution.py:338
  124.3 2.8 %collective-permute-start.43 = (bf16[32,2048]{1,0:T(8,128)(2,1)S(1)}, bf16[32,2048]{1,0:T(8,128)(2,1)S(1)}, u32[]{:S(2)}, u32[]{:S(2)}) collective-permute-start(bf16[32,2048]{1,0:T(8,128)(2,1)S(1)} %get-tuple-element.114), channel_id=1, source_target_pairs={{0,10},{2,8},{4,14},{6,12},{8,2},{10,0},{12,6},{14,4},{16,26},{18,... | collective-permute-start | bytes 393224 | tf_op jit(solution)/shard_map/ppermute | solution.py:338
  127.1 4.2 %collective-permute-start.44 = (bf16[32,2048]{1,0:T(8,128)(2,1)S(1)}, bf16[32,2048]{1,0:T(8,128)(2,1)S(1)}, u32[]{:S(2)}, u32[]{:S(2)}) collective-permute-start(bf16[32,2048]{1,0:T(8,128)(2,1)S(1)} %get-tuple-element.115), channel_id=1, source_target_pairs={{0,12},{2,14},{4,8},{6,10},{8,4},{10,6},{12,0},{14,2},{16,28},{18,... | collective-permute-start | bytes 393224 | tf_op jit(solution)/shard_map/ppermute | solution.py:338
  131.3 2.7 %collective-permute-done.21.refs_7_ = bf16[32,2048]{1,0:T(8,128)(2,1)S(1)} collective-permute-done((bf16[32,2048]{1,0:T(8,128)(2,1)S(1)}, bf16[32,2048]{1,0:T(8,128)(2,1)S(1)}, u32[]{:S(2)}, u32[]{:S(2)}) %collective-permute-start.21) | collective-permute-done | bytes 131104 | tf_op jit(solution)/shard_map/ppermute | solution.py:338
  139.4 5.6 %collective-permute-start.34 = (bf16[32,2048]{1,0:T(8,128)(2,1)S(1)}, bf16[32,2048]{1,0:T(8,128)(2,1)S(1)}, u32[]{:S(2)}, u32[]{:S(2)}) collective-permute-start(bf16[32,2048]{1,0:T(8,128)(2,1)S(1)} %get-tuple-element.104), channel_id=1, source_target_pairs={{0,22},{2,20},{4,18},{6,16},{8,30},{10,28},{12,26},{14,24},{16,6},... | collective-permute-start | bytes 393224 | tf_op jit(solution)/shard_map/ppermute | solution.py:338
  145.0 2.1 %collective-permute-start.35 = (bf16[32,2048]{1,0:T(8,128)(2,1)S(1)}, bf16[32,2048]{1,0:T(8,128)(2,1)S(1)}, u32[]{:S(2)}, u32[]{:S(2)}) collective-permute-start(bf16[32,2048]{1,0:T(8,128)(2,1)S(1)} %get-tuple-element.105), channel_id=1, source_target_pairs={{0,28},{2,30},{4,24},{6,26},{8,20},{10,22},{12,16},{14,18},{16,12}... | collective-permute-start | bytes 393224 | tf_op jit(solution)/shard_map/ppermute | solution.py:338
  147.1 2.4 %collective-permute-done.39.refs_11_ = bf16[32,2048]{1,0:T(8,128)(2,1)S(1)} collective-permute-done((bf16[32,2048]{1,0:T(8,128)(2,1)S(1)}, bf16[32,2048]{1,0:T(8,128)(2,1)S(1)}, u32[]{:S(2)}, u32[]{:S(2)}) %collective-permute-start.39) | collective-permute-done | bytes 131104 | tf_op jit(solution)/shard_map/ppermute | solution.py:338
  150.9 5.3 %collective-permute-done.34.refs_6_ = bf16[32,2048]{1,0:T(8,128)(2,1)S(1)} collective-permute-done((bf16[32,2048]{1,0:T(8,128)(2,1)S(1)}, bf16[32,2048]{1,0:T(8,128)(2,1)S(1)}, u32[]{:S(2)}, u32[]{:S(2)}) %collective-permute-start.34) | collective-permute-done | bytes 131104 | tf_op jit(solution)/shard_map/ppermute | solution.py:338
  156.2 2.9 %collective-permute-done.35.refs_7_ = bf16[32,2048]{1,0:T(8,128)(2,1)S(1)} collective-permute-done((bf16[32,2048]{1,0:T(8,128)(2,1)S(1)}, bf16[32,2048]{1,0:T(8,128)(2,1)S(1)}, u32[]{:S(2)}, u32[]{:S(2)}) %collective-permute-start.35) | collective-permute-done | bytes 131104 | tf_op jit(solution)/shard_map/ppermute | solution.py:338
  159.0 4.5 %collective-permute-done.36.refs_8_ = bf16[32,2048]{1,0:T(8,128)(2,1)S(1)} collective-permute-done((bf16[32,2048]{1,0:T(8,128)(2,1)S(1)}, bf16[32,2048]{1,0:T(8,128)(2,1)S(1)}, u32[]{:S(2)}, u32[]{:S(2)}) %collective-permute-start.36) | collective-permute-done | bytes 131104 | tf_op jit(solution)/shard_map/ppermute | solution.py:338
  163.5 2.2 %shard_map.204 = bf16[128,2048]{1,0:T(8,128)(2,1)} custom-call(f32[128,2048]{1,0:T(8,128)S(1)} %shard_map.197.refs_0_, bf16[128,512]{1,0:T(8,128)(2,1)S(1)} %get-tuple-element.71.refs_11_.refs_1_, bf16[128,512]{1,0:T(8,128)(2,1)S(1)} %get-tuple-element.72.refs_12_.refs_2_, f32[2,128]{1,0:T(2,128)S(1)} %bitcast.10, f32[1,2048]{1,0:T(1,128)S(1)} %bitcast.8, ...), custom_call_target="tpu_custom_call" | custom-call | flops 402653184 | bytes 1048576 | tf_op jit(solution)/shard_map/pallas_call | solution.py:50
  (103 shorter events, 31.4 us)
Async XLA Ops:
  0.0 19.2 %collective-permute-start.7 = (bf16[512,2048]{1,0:T(8,128)(2,1)}, bf16[512,2048]{1,0:T(8,128)(2,1)S(1)}, u32[]{:S(2)}, u32[]{:S(2)}) collective-permute-start(bf16[512,2048]{1,0:T(8,128)(2,1)} %refs_7_.3), channel_id=1, source_target_pairs={{0,1},{1,0},{2,3},{3,2},{4,5},{5,4},{6,7},{7,6},{8,9},{9,8},{10,11... | collective-permute-start | bytes 6291464 | tf_op jit(solution)/shard_map/ppermute | solution.py:333
  4.0 9.0 %collective-permute-start = (bf16[128,384]{1,0:T(8,128)(2,1)S(1)}, bf16[128,384]{1,0:T(8,128)(2,1)S(1)}, u32[]{:S(2)}, u32[]{:S(2)}) collective-permute-start(bf16[128,384]{1,0:T(8,128)(2,1)S(1)} %get-tuple-element.62), channel_id=1, source_target_pairs={{0,8},{2,10},{4,12},{6,14},{8,16},{10,18},{12,20},{14,22},{16,24},... | collective-permute-start | bytes 294920 | tf_op jit(solution)/shard_map/ppermute | solution.py:349
  8.2 9.2 %collective-permute-start.3 = (bf16[128,384]{1,0:T(8,128)(2,1)S(1)}, bf16[128,384]{1,0:T(8,128)(2,1)S(1)}, u32[]{:S(2)}, u32[]{:S(2)}) collective-permute-start(bf16[128,384]{1,0:T(8,128)(2,1)S(1)} %get-tuple-element.62), channel_id=1, source_target_pairs={{0,2},{2,4},{4,6},{6,8},{8,10},{10,12},{12,14},{14,16},{16,18},{18... | collective-permute-start | bytes 294920 | tf_op jit(solution)/shard_map/ppermute | solution.py:349
  29.4 27.6 %collective-permute-start.13 = (bf16[32,2048]{1,0:T(8,128)(2,1)S(1)}, bf16[32,2048]{1,0:T(8,128)(2,1)S(1)}, u32[]{:S(2)}, u32[]{:S(2)}) collective-permute-start(bf16[32,2048]{1,0:T(8,128)(2,1)S(1)} %get-tuple-element.82), channel_id=1, source_target_pairs={{0,2},{2,0},{4,6},{6,4},{8,10},{10,8},{12,14},{14,12},{16,18},{18,... | collective-permute-start | bytes 393224 | tf_op jit(solution)/shard_map/ppermute | solution.py:338
  29.5 28.5 %collective-permute-start.14 = (bf16[32,2048]{1,0:T(8,128)(2,1)S(1)}, bf16[32,2048]{1,0:T(8,128)(2,1)S(1)}, u32[]{:S(2)}, u32[]{:S(2)}) collective-permute-start(bf16[32,2048]{1,0:T(8,128)(2,1)S(1)} %get-tuple-element.83), channel_id=1, source_target_pairs={{0,4},{2,6},{4,0},{6,2},{8,12},{10,14},{12,8},{14,10},{16,20},{18,... | collective-permute-start | bytes 393224 | tf_op jit(solution)/shard_map/ppermute | solution.py:338
  29.7 34.8 %collective-permute-start.15 = (bf16[32,2048]{1,0:T(8,128)(2,1)S(1)}, bf16[32,2048]{1,0:T(8,128)(2,1)S(1)}, u32[]{:S(2)}, u32[]{:S(2)}) collective-permute-start(bf16[32,2048]{1,0:T(8,128)(2,1)S(1)} %get-tuple-element.84), channel_id=1, source_target_pairs={{0,6},{2,4},{4,2},{6,0},{8,14},{10,12},{12,10},{14,8},{16,22},{18,... | collective-permute-start | bytes 393224 | tf_op jit(solution)/shard_map/ppermute | solution.py:338
  33.0 9.4 %collective-permute-start.8 = (bf16[32,2048]{1,0:T(8,128)(2,1)S(1)}, bf16[32,2048]{1,0:T(8,128)(2,1)S(1)}, u32[]{:S(2)}, u32[]{:S(2)}) collective-permute-start(bf16[32,2048]{1,0:T(8,128)(2,1)S(1)} %get-tuple-element.74), channel_id=1, source_target_pairs={{0,16},{2,18},{4,20},{6,22},{8,24},{10,26},{12,28},{14,30},{16,0},... | collective-permute-start | bytes 393224 | tf_op jit(solution)/shard_map/ppermute | solution.py:338
  35.2 29.4 %collective-permute-start.9 = (bf16[32,2048]{1,0:T(8,128)(2,1)S(1)}, bf16[32,2048]{1,0:T(8,128)(2,1)S(1)}, u32[]{:S(2)}, u32[]{:S(2)}) collective-permute-start(bf16[32,2048]{1,0:T(8,128)(2,1)S(1)} %get-tuple-element.75), channel_id=1, source_target_pairs={{0,18},{2,16},{4,22},{6,20},{8,26},{10,24},{12,30},{14,28},{16,2},... | collective-permute-start | bytes 393224 | tf_op jit(solution)/shard_map/ppermute | solution.py:338
  56.0 12.0 %collective-permute-start.10 = (bf16[32,2048]{1,0:T(8,128)(2,1)S(1)}, bf16[32,2048]{1,0:T(8,128)(2,1)S(1)}, u32[]{:S(2)}, u32[]{:S(2)}) collective-permute-start(bf16[32,2048]{1,0:T(8,128)(2,1)S(1)} %get-tuple-element.76), channel_id=1, source_target_pairs={{0,24},{2,26},{4,28},{6,30},{8,16},{10,18},{12,20},{14,22},{16,8},... | collective-permute-start | bytes 393224 | tf_op jit(solution)/shard_map/ppermute | solution.py:338
  57.1 12.7 %collective-permute-start.11 = (bf16[32,2048]{1,0:T(8,128)(2,1)S(1)}, bf16[32,2048]{1,0:T(8,128)(2,1)S(1)}, u32[]{:S(2)}, u32[]{:S(2)}) collective-permute-start(bf16[32,2048]{1,0:T(8,128)(2,1)S(1)} %get-tuple-element.77), channel_id=1, source_target_pairs={{0,26},{2,24},{4,30},{6,28},{8,18},{10,16},{12,22},{14,20},{16,10}... | collective-permute-start | bytes 393224 | tf_op jit(solution)/shard_map/ppermute | solution.py:338
  58.0 15.3 %collective-permute-start.28 = (bf16[32,2048]{1,0:T(8,128)(2,1)S(1)}, bf16[32,2048]{1,0:T(8,128)(2,1)S(1)}, u32[]{:S(2)}, u32[]{:S(2)}) collective-permute-start(bf16[32,2048]{1,0:T(8,128)(2,1)S(1)} %get-tuple-element.97), channel_id=1, source_target_pairs={{0,10},{2,8},{4,14},{6,12},{8,2},{10,0},{12,6},{14,4},{16,26},{18,... | collective-permute-start | bytes 393224 | tf_op jit(solution)/shard_map/ppermute | solution.py:338
  64.5 11.1 %collective-permute-start.29 = (bf16[32,2048]{1,0:T(8,128)(2,1)S(1)}, bf16[32,2048]{1,0:T(8,128)(2,1)S(1)}, u32[]{:S(2)}, u32[]{:S(2)}) collective-permute-start(bf16[32,2048]{1,0:T(8,128)(2,1)S(1)} %get-tuple-element.98), channel_id=1, source_target_pairs={{0,12},{2,14},{4,8},{6,10},{8,4},{10,6},{12,0},{14,2},{16,28},{18,... | collective-permute-start | bytes 393224 | tf_op jit(solution)/shard_map/ppermute | solution.py:338
  64.6 15.0 %collective-permute-start.30 = (bf16[32,2048]{1,0:T(8,128)(2,1)S(1)}, bf16[32,2048]{1,0:T(8,128)(2,1)S(1)}, u32[]{:S(2)}, u32[]{:S(2)}) collective-permute-start(bf16[32,2048]{1,0:T(8,128)(2,1)S(1)} %get-tuple-element.99), channel_id=1, source_target_pairs={{0,14},{2,12},{4,10},{6,8},{8,6},{10,4},{12,2},{14,0},{16,30},{18,... | collective-permute-start | bytes 393224 | tf_op jit(solution)/shard_map/ppermute | solution.py:338
  67.9 24.3 %collective-permute-start.23 = (bf16[32,2048]{1,0:T(8,128)(2,1)S(1)}, bf16[32,2048]{1,0:T(8,128)(2,1)S(1)}, u32[]{:S(2)}, u32[]{:S(2)}) collective-permute-start(bf16[32,2048]{1,0:T(8,128)(2,1)S(1)} %get-tuple-element.93), channel_id=1, source_target_pairs={{0,22},{2,20},{4,18},{6,16},{8,30},{10,28},{12,26},{14,24},{16,6},... | collective-permute-start | bytes 393224 | tf_op jit(solution)/shard_map/ppermute | solution.py:338
  69.8 22.5 %collective-permute-start.24 = (bf16[32,2048]{1,0:T(8,128)(2,1)S(1)}, bf16[32,2048]{1,0:T(8,128)(2,1)S(1)}, u32[]{:S(2)}, u32[]{:S(2)}) collective-permute-start(bf16[32,2048]{1,0:T(8,128)(2,1)S(1)} %get-tuple-element.94), channel_id=1, source_target_pairs={{0,28},{2,30},{4,24},{6,26},{8,20},{10,22},{12,16},{14,18},{16,12}... | collective-permute-start | bytes 393224 | tf_op jit(solution)/shard_map/ppermute | solution.py:338
  75.6 16.7 %collective-permute-start.25 = (bf16[32,2048]{1,0:T(8,128)(2,1)S(1)}, bf16[32,2048]{1,0:T(8,128)(2,1)S(1)}, u32[]{:S(2)}, u32[]{:S(2)}) collective-permute-start(bf16[32,2048]{1,0:T(8,128)(2,1)S(1)} %get-tuple-element.95), channel_id=1, source_target_pairs={{0,30},{2,28},{4,26},{6,24},{8,22},{10,20},{12,18},{14,16},{16,14}... | collective-permute-start | bytes 393224 | tf_op jit(solution)/shard_map/ppermute | solution.py:338
  79.6 14.7 %collective-permute-start.31 = (bf16[128,2048]{1,0:T(8,128)(2,1)S(1)}, bf16[128,2048]{1,0:T(8,128)(2,1)S(1)}, u32[]{:S(2)}, u32[]{:S(2)}) collective-permute-start(bf16[128,2048]{1,0:T(8,128)(2,1)S(1)} %constant_dynamic-update-slice_fusion.16.refs_0_), channel_id=1, source_target_pairs={{0,1},{1,0},{2,3},{3,2},{4,5},{5,4},{6,7},{7,6},{8,9},{9,8},{10,11... | collective-permute-start | bytes 1572872 | tf_op jit(solution)/shard_map/ppermute | solution.py:333
  92.3 8.2 %collective-permute-start.26 = (bf16[128,2048]{1,0:T(8,128)(2,1)S(1)}, bf16[128,2048]{1,0:T(8,128)(2,1)S(1)}, u32[]{:S(2)}, u32[]{:S(2)}) collective-permute-start(bf16[128,2048]{1,0:T(8,128)(2,1)S(1)} %constant_dynamic-update-slice_fusion.12.refs_0_), channel_id=1, source_target_pairs={{0,1},{1,0},{2,3},{3,2},{4,5},{5,4},{6,7},{7,6},{8,9},{9,8},{10,11... | collective-permute-start | bytes 1572872 | tf_op jit(solution)/shard_map/ppermute | solution.py:333
  107.2 17.0 %collective-permute-start.18 = (bf16[32,2048]{1,0:T(8,128)(2,1)S(1)}, bf16[32,2048]{1,0:T(8,128)(2,1)S(1)}, u32[]{:S(2)}, u32[]{:S(2)}) collective-permute-start(bf16[32,2048]{1,0:T(8,128)(2,1)S(1)} %get-tuple-element.88.refs_1_), channel_id=1, source_target_pairs={{0,16},{2,18},{4,20},{6,22},{8,24},{10,26},{12,28},{14,30},{16,0},... | collective-permute-start | bytes 393224 | tf_op jit(solution)/shard_map/ppermute | solution.py:338
  110.0 17.1 %collective-permute-start.19 = (bf16[32,2048]{1,0:T(8,128)(2,1)S(1)}, bf16[32,2048]{1,0:T(8,128)(2,1)S(1)}, u32[]{:S(2)}, u32[]{:S(2)}) collective-permute-start(bf16[32,2048]{1,0:T(8,128)(2,1)S(1)} %get-tuple-element.89), channel_id=1, source_target_pairs={{0,18},{2,16},{4,22},{6,20},{8,26},{10,24},{12,30},{14,28},{16,2},... | collective-permute-start | bytes 393224 | tf_op jit(solution)/shard_map/ppermute | solution.py:338
  110.2 21.0 %collective-permute-start.20 = (bf16[32,2048]{1,0:T(8,128)(2,1)S(1)}, bf16[32,2048]{1,0:T(8,128)(2,1)S(1)}, u32[]{:S(2)}, u32[]{:S(2)}) collective-permute-start(bf16[32,2048]{1,0:T(8,128)(2,1)S(1)} %get-tuple-element.90), channel_id=1, source_target_pairs={{0,24},{2,26},{4,28},{6,30},{8,16},{10,18},{12,20},{14,22},{16,8},... | collective-permute-start | bytes 393224 | tf_op jit(solution)/shard_map/ppermute | solution.py:338
  111.8 22.1 %collective-permute-start.21 = (bf16[32,2048]{1,0:T(8,128)(2,1)S(1)}, bf16[32,2048]{1,0:T(8,128)(2,1)S(1)}, u32[]{:S(2)}, u32[]{:S(2)}) collective-permute-start(bf16[32,2048]{1,0:T(8,128)(2,1)S(1)} %get-tuple-element.91), channel_id=1, source_target_pairs={{0,26},{2,24},{4,30},{6,28},{8,18},{10,16},{12,22},{14,20},{16,10}... | collective-permute-start | bytes 393224 | tf_op jit(solution)/shard_map/ppermute | solution.py:338
  113.4 21.8 %collective-permute-start.42 = (bf16[32,2048]{1,0:T(8,128)(2,1)S(1)}, bf16[32,2048]{1,0:T(8,128)(2,1)S(1)}, u32[]{:S(2)}, u32[]{:S(2)}) collective-permute-start(bf16[32,2048]{1,0:T(8,128)(2,1)S(1)} %get-tuple-element.113), channel_id=1, source_target_pairs={{0,8},{2,10},{4,12},{6,14},{8,0},{10,2},{12,4},{14,6},{16,24},{18,... | collective-permute-start | bytes 393224 | tf_op jit(solution)/shard_map/ppermute | solution.py:338
  124.3 12.0 %collective-permute-start.43 = (bf16[32,2048]{1,0:T(8,128)(2,1)S(1)}, bf16[32,2048]{1,0:T(8,128)(2,1)S(1)}, u32[]{:S(2)}, u32[]{:S(2)}) collective-permute-start(bf16[32,2048]{1,0:T(8,128)(2,1)S(1)} %get-tuple-element.114), channel_id=1, source_target_pairs={{0,10},{2,8},{4,14},{6,12},{8,2},{10,0},{12,6},{14,4},{16,26},{18,... | collective-permute-start | bytes 393224 | tf_op jit(solution)/shard_map/ppermute | solution.py:338
  127.1 10.5 %collective-permute-start.44 = (bf16[32,2048]{1,0:T(8,128)(2,1)S(1)}, bf16[32,2048]{1,0:T(8,128)(2,1)S(1)}, u32[]{:S(2)}, u32[]{:S(2)}) collective-permute-start(bf16[32,2048]{1,0:T(8,128)(2,1)S(1)} %get-tuple-element.115), channel_id=1, source_target_pairs={{0,12},{2,14},{4,8},{6,10},{8,4},{10,6},{12,0},{14,2},{16,28},{18,... | collective-permute-start | bytes 393224 | tf_op jit(solution)/shard_map/ppermute | solution.py:338
  133.9 11.0 %collective-permute-start.38 = (bf16[32,2048]{1,0:T(8,128)(2,1)S(1)}, bf16[32,2048]{1,0:T(8,128)(2,1)S(1)}, u32[]{:S(2)}, u32[]{:S(2)}) collective-permute-start(bf16[32,2048]{1,0:T(8,128)(2,1)S(1)} %get-tuple-element.109), channel_id=1, source_target_pairs={{0,2},{2,0},{4,6},{6,4},{8,10},{10,8},{12,14},{14,12},{16,18},{18,... | collective-permute-start | bytes 393224 | tf_op jit(solution)/shard_map/ppermute | solution.py:338
  135.2 14.2 %collective-permute-start.39 = (bf16[32,2048]{1,0:T(8,128)(2,1)S(1)}, bf16[32,2048]{1,0:T(8,128)(2,1)S(1)}, u32[]{:S(2)}, u32[]{:S(2)}) collective-permute-start(bf16[32,2048]{1,0:T(8,128)(2,1)S(1)} %get-tuple-element.110), channel_id=1, source_target_pairs={{0,4},{2,6},{4,0},{6,2},{8,12},{10,14},{12,8},{14,10},{16,20},{18,... | collective-permute-start | bytes 393224 | tf_op jit(solution)/shard_map/ppermute | solution.py:338
  136.2 14.6 %collective-permute-start.33 = (bf16[32,2048]{1,0:T(8,128)(2,1)S(1)}, bf16[32,2048]{1,0:T(8,128)(2,1)S(1)}, u32[]{:S(2)}, u32[]{:S(2)}) collective-permute-start(bf16[32,2048]{1,0:T(8,128)(2,1)S(1)} %get-tuple-element.103.refs_2_), channel_id=1, source_target_pairs={{0,20},{2,22},{4,16},{6,18},{8,28},{10,30},{12,24},{14,26},{16,4},... | collective-permute-start | bytes 393224 | tf_op jit(solution)/shard_map/ppermute | solution.py:338
  137.5 13.3 %collective-permute-start.40 = (bf16[32,2048]{1,0:T(8,128)(2,1)S(1)}, bf16[32,2048]{1,0:T(8,128)(2,1)S(1)}, u32[]{:S(2)}, u32[]{:S(2)}) collective-permute-start(bf16[32,2048]{1,0:T(8,128)(2,1)S(1)} %get-tuple-element.111), channel_id=1, source_target_pairs={{0,6},{2,4},{4,2},{6,0},{8,14},{10,12},{12,10},{14,8},{16,22},{18,... | collective-permute-start | bytes 393224 | tf_op jit(solution)/shard_map/ppermute | solution.py:338
  139.4 16.8 %collective-permute-start.34 = (bf16[32,2048]{1,0:T(8,128)(2,1)S(1)}, bf16[32,2048]{1,0:T(8,128)(2,1)S(1)}, u32[]{:S(2)}, u32[]{:S(2)}) collective-permute-start(bf16[32,2048]{1,0:T(8,128)(2,1)S(1)} %get-tuple-element.104), channel_id=1, source_target_pairs={{0,22},{2,20},{4,18},{6,16},{8,30},{10,28},{12,26},{14,24},{16,6},... | collective-permute-start | bytes 393224 | tf_op jit(solution)/shard_map/ppermute | solution.py:338
  145.0 14.1 %collective-permute-start.35 = (bf16[32,2048]{1,0:T(8,128)(2,1)S(1)}, bf16[32,2048]{1,0:T(8,128)(2,1)S(1)}, u32[]{:S(2)}, u32[]{:S(2)}) collective-permute-start(bf16[32,2048]{1,0:T(8,128)(2,1)S(1)} %get-tuple-element.105), channel_id=1, source_target_pairs={{0,28},{2,30},{4,24},{6,26},{8,20},{10,22},{12,16},{14,18},{16,12}... | collective-permute-start | bytes 393224 | tf_op jit(solution)/shard_map/ppermute | solution.py:338
  149.4 14.1 %collective-permute-start.36 = (bf16[32,2048]{1,0:T(8,128)(2,1)S(1)}, bf16[32,2048]{1,0:T(8,128)(2,1)S(1)}, u32[]{:S(2)}, u32[]{:S(2)}) collective-permute-start(bf16[32,2048]{1,0:T(8,128)(2,1)S(1)} %get-tuple-element.106), channel_id=1, source_target_pairs={{0,30},{2,28},{4,26},{6,24},{8,22},{10,20},{12,18},{14,16},{16,14}... | collective-permute-start | bytes 393224 | tf_op jit(solution)/shard_map/ppermute | solution.py:338
  (16 other events, 189.7 us)

commit v3 on v2

--- a/solution.py
+++ b/solution.py
@@ -20,6 +20,7 @@
 RESIDUAL_SCALE = 2.0**0.5
 NORM_EPSILON = 1e-05
 LANES = 128
+CARRIED = 5
 FAR = 2.0**24
 F32 = jnp.float32
 BF16 = jnp.bfloat16
@@ -103,9 +104,11 @@
     send[...] = own[part, :]
 
 
-def ready_kernel(where, content, content_far, turning, turning_far, docs, routes, nc, ns, bc, bs, down, queries, pick0, pick1, down_held, sem, *, capacity):
-    copy = pltpu.make_async_copy(down, down_held, sem)
-    copy.start()
+def ready_kernel(where, content, content_far, turning, turning_far, docs, routes, nc, ns, bc, bs, *refs, capacity):
+    carried, queries, pick0, pick1, held, sems = refs[:CARRIED], *refs[CARRIED : CARRIED + 3], refs[CARRIED + 3 : -1], refs[-1]
+    copies = [pltpu.make_async_copy(a, b, sems.at[k]) for k, (a, b) in enumerate(zip(carried, held))]
+    for copy in copies:
+        copy.start()
     sp, tp = where[0], where[1]
     rows = content.shape[0]
     heads_here = HEADS // 2
@@ -141,7 +144,8 @@
     for route, pick in ((first, pick0), (second, pick1)):
         place = jnp.sum(jnp.where(route == lane, rank, 0.0), 1, keepdims=True).astype(jnp.int32)
         pick[...] = (slot == (route ^ sp) * capacity + place).astype(BF16)
-    copy.wait()
+    for copy in copies:
+        copy.wait()
 
 
 def layer_norm(values, gain):
@@ -158,13 +162,12 @@
     ]
     normed, gate_held, up_held = refs[12 + near : 15 + near]
     outbound = refs[15 + near : 15 + near + pieces]
-    packed, keys, values, attended, summed, w_mine, w_theirs, sems = refs[15 + near + pieces :]
+    packed, keys, values, attended, summed, w_mine, sems = refs[15 + near + pieces :]
     tp = where[1]
     copies = [
         pltpu.make_async_copy(out_mine, w_mine, sems.at[0]),
-        pltpu.make_async_copy(out_theirs, w_theirs, sems.at[1]),
-        pltpu.make_async_copy(gate, gate_held, sems.at[2]),
-        pltpu.make_async_copy(up, up_held, sems.at[3]),
+        pltpu.make_async_copy(gate, gate_held, sems.at[1]),
+        pltpu.make_async_copy(up, up_held, sems.at[2]),
     ]
     for copy in copies:
         copy.start()
@@ -202,8 +205,7 @@
     half = w_mine.shape[0]
     copies[0].wait()
     summed[...] = dot(attended[:, :half], w_mine[...]).astype(BF16).astype(F32)
-    copies[1].wait()
-    summed[...] += dot(attended[:, half:], w_theirs[...]).astype(BF16).astype(F32)
+    summed[...] += dot(attended[:, half:], out_theirs[...]).astype(BF16).astype(F32)
     step = 32
 
     def norm_step(k, carry):
@@ -217,8 +219,8 @@
     placed = dot(both, normed[...], ((0,), (0,))).astype(BF16)
     for k, ref in enumerate(outbound):
         ref[...] = placed[k * capacity : (k + 1) * capacity]
+    copies[1].wait()
     copies[2].wait()
-    copies[3].wait()
 
 
 def expert_kernel(own, other, w_gate, w_up, w_down, mine, theirs):
@@ -297,8 +299,9 @@
 
 def group_order(chips):
     order = np.arange(chips).reshape(4, chips // 4)
-    half = chips // 8
-    groups = [order[2:, :half], order[2:, half:], order[1], order[0]]
+    beyond = order[2:].T.reshape(-1)
+    cut = chips // 4
+    groups = [beyond[:cut], beyond[cut:], order[1], order[0]]
     return [[int(s) for s in group.reshape(-1)] for group in groups]
 
 
@@ -359,34 +362,35 @@
         return mine, across(lax.dynamic_slice_in_dim(value, (1 - tp) * rows, rows, 0))
 
     args = [where, *split(queries_content), *split(queries_rotary), far(docs), far(routes.T)]
-    args += [*map(far, tables), far(w_down)]
-    queries_ready, pick0, pick1, w_down = call(
+    carried = [w_key_up, w_value_up, residual, norm_gain.reshape(1, width), w_down]
+    args += [*map(far, tables), *map(far, carried)]
+    queries_ready, pick0, pick1, w_key_up, w_value_up, residual, norm_gain, w_down = call(
         functools.partial(ready_kernel, capacity=capacity),
         [
             shape(rows, HEADS * 256),
             shape(rows, chips * capacity),
             shape(rows, chips * capacity),
-            shape(*w_down.shape),
+            *[shape(*value.shape, dtype=value.dtype) for value in carried],
         ],
         args,
         1 << 26,
         scalars=1,
-        hbm=(len(args) - 1,),
-        scratch=[pltpu.SemaphoreType.DMA],
+        hbm=range(len(args) - CARRIED, len(args)),
+        scratch=[pltpu.SemaphoreType.DMA((CARRIED,))],
     )
     kv_near, queries_ready = lax.optimization_barrier((kv_near, queries_ready))
     kv_all = [jnp.concatenate(kv_near, 0)]
     kv_all.append(across(kv_all[0]))
     reach = tok_dev + sum(value.shape[0] for value in kv_all)
-    args = [where, kv_own, *kv_all, queries_ready, far(w_key_up), far(w_value_up), far(w_out), out_theirs]
-    hbm = (len(args) - 2, len(args) - 1, len(args) + 4, len(args) + 5)
-    args += [far(residual), far(norm_gain.reshape(1, width)), pick0, pick1, far(w_gate), far(w_up)]
+    args = [where, kv_own, *kv_all, queries_ready, w_key_up, w_value_up, far(w_out), out_theirs]
+    hbm = (len(args) - 2, len(args) + 4, len(args) + 5)
+    args += [residual, norm_gain, pick0, pick1, far(w_gate), far(w_up)]
     normed, w_gate, w_up, *outbound = call(
         functools.partial(attend_kernel, near=len(kv_all), pieces=chips, capacity=capacity),
         [shape(rows, width), shape(*w_gate.shape), shape(*w_up.shape)] + [shape(capacity, width)] * chips,
         args,
         1 << 32,
-        limit=20,
+        limit=18,
         scalars=1,
         hbm=hbm,
         scratch=[
@@ -396,8 +400,7 @@
             pltpu.VMEM((rows, HEADS * DV), BF16),
             pltpu.VMEM((rows, width), F32),
             pltpu.VMEM(w_out.shape, BF16),
-            pltpu.VMEM(w_out.shape, BF16),
-            pltpu.SemaphoreType.DMA((4,)),
+            pltpu.SemaphoreType.DMA((3,)),
         ],
     )
     groups = group_order(chips)
@@ -439,12 +442,12 @@
     marked = mark(give_back(far_a)[0])
     mine, theirs = work(next_plane, marked)
     halves[next_plane] = (mine, across(theirs))
-    mine, theirs = work(far_b, mine)
+    given = give_back(plane, mine)[0]
+    mine, theirs = work(far_b, mine, given)
     halves[far_b] = (mine, across(theirs))
     last = give_back(far_b)[0]
-    give_back(plane, last)
     give_back(next_plane, last)
-    early, late = groups[far_a], groups[far_b] + groups[plane] + groups[next_plane]
+    early, late = groups[far_a] + groups[plane], groups[far_b] + groups[next_plane]
 
     def gathered(total, pieces, body, out, extra=()):
         return call(

time: 166 us -> 188 us (1.13)
  waiting for transfers between devices: 53.6 us -> 71.6 us
  starting transfers between devices: 66.2 us -> 70.1 us
    ppermute x30, waiting for transfers between devices: 46.3 us -> 65 us  [exchange(): return lax.ppermute(value, 'sp', [(j, j ^ s) for j in range(chips)])]
    ppermute x30, starting transfers between devices: 58.7 us -> 62.6 us  [exchange(): return lax.ppermute(value, 'sp', [(j, j ^ s) for j in range(chips)])]
  transfers between devices with their start and end apart: 46 -> 46, of which waited for: 17 -> 21; matrix products, arithmetic and copies ran while one was open for 1% -> 1% of each run, Pallas kernels for 15% -> 14%
where the time goes in v3:
time: 188 us; the launch traced here: 187 us
  waiting for transfers between devices  71.6 us (38%)
  starting transfers between devices  70.1 us (37%)
  Pallas kernels  42.5 us (23%)
  local copies, waits for them, and re-layouts  2.11 us (1%)
    ppermute x30, waiting for transfers between devices, exchange(): return lax.ppermute(value, 'sp', [(j, j ^ s) for j in range(chips)])  65 us
    ppermute x30, starting transfers between devices, exchange(): return lax.ppermute(value, 'sp', [(j, j ^ s) for j in range(chips)])  62.6 us
    pallas_call x15, Pallas kernels, call(): pl.pallas_call(ordered, out_shape=outs, in_specs=specs, out_specs=jax.tre...  42.5 us
    ppermute x4, starting transfers between devices, per_device(): lax.ppermute(kv_send, 'sp', [(j, (j + d) % chips) for j in range(chips)])  4.82 us
  transfers between devices with their start and end apart: 46, of which 21 were waited for; matrix products, arithmetic and copies ran while one was open for 1% of the time, Pallas kernels for 14%

profile of v3, /device:TPU:16, one launch (start us, length us, event | category | flops | bytes accessed | tf_op | source)
XLA Modules:
  0.0 186.7 jit_solution(17097271818092597748)
XLA Ops:
  5.6 2.4 %collective-permute-start.1 = (bf16[128,384]{1,0:T(8,128)(2,1)S(1)}, bf16[128,384]{1,0:T(8,128)(2,1)S(1)}, u32[]{:S(2)}, u32[]{:S(2)}) collective-permute-start(bf16[128,384]{1,0:T(8,128)(2,1)S(1)} %get-tuple-element.66), channel_id=1, source_target_pairs={{0,6},{2,8},{4,10},{6,12},{8,14},{10,16},{12,18},{14,20},{16,22},{... | collective-permute-start | bytes 294920 | tf_op jit(solution)/shard_map/ppermute | solution.py:352
  8.8 4.8 %shard_map.191 = (bf16[128,2048]{1,0:T(8,128)(2,1)S(1)}, bf16[128,512]{1,0:T(8,128)(2,1)S(1)}, bf16[128,512]{1,0:T(8,128)(2,1)S(1)}, bf16[256,1024]{1,0:T(8,128)...) custom-call(s32[2]{0:T(128)S(1)} %pad_add_fusion.refs_0_, ...), custom_call_target="tpu_custom_call" | custom-call | flops 67108864 | bytes 1048576 | tf_op jit(solution)/shard_map/pallas_call | solution.py:51
  14.4 3.0 %collective-permute-done.3 = bf16[128,384]{1,0:T(8,128)(2,1)S(1)} collective-permute-done((bf16[128,384]{1,0:T(8,128)(2,1)S(1)}, bf16[128,384]{1,0:T(8,128)(2,1)S(1)}, u32[]{:S(2)}, u32[]{:S(2)}) %collective-permute-start.3) | collective-permute-done | bytes 98336 | tf_op jit(solution)/shard_map/ppermute | solution.py:352
  19.2 9.1 %shard_map.192 = (bf16[128,2048]{1,0:T(8,128)(2,1)S(1)}, bf16[1,2048,1792]{2,1,0:T(8,128)(2,1)S(1)}, bf16[1,2048,1792]{2,1,0:T(8,128)(2,1)S(1)}, bf16[32,2048]{1...) custom-call(s32[2]{0:T(128)S(1)} %pad_add_fusion.refs_0_, ...), custom_call_target="tpu_custom_call" | custom-call | flops 4294967296 | bytes 1048576 | tf_op jit(solution)/shard_map/pallas_call | solution.py:51
  28.4 3.9 %collective-permute-start.32 = (bf16[32,2048]{1,0:T(8,128)(2,1)S(1)}, bf16[32,2048]{1,0:T(8,128)(2,1)S(1)}, u32[]{:S(2)}, u32[]{:S(2)}) collective-permute-start(bf16[32,2048]{1,0:T(8,128)(2,1)S(1)} %get-tuple-element.111), channel_id=1, source_target_pairs={{0,28},{2,30},{4,24},{6,26},{8,20},{10,22},{12,16},{14,18},{16,12}... | collective-permute-start | bytes 393224 | tf_op jit(solution)/shard_map/ppermute | solution.py:341
  32.6 4.3 %collective-permute-start.34 = (bf16[32,2048]{1,0:T(8,128)(2,1)S(1)}, bf16[32,2048]{1,0:T(8,128)(2,1)S(1)}, u32[]{:S(2)}, u32[]{:S(2)}) collective-permute-start(bf16[32,2048]{1,0:T(8,128)(2,1)S(1)} %get-tuple-element.113), channel_id=1, source_target_pairs={{0,30},{2,28},{4,26},{6,24},{8,22},{10,20},{12,18},{14,16},{16,14}... | collective-permute-start | bytes 393224 | tf_op jit(solution)/shard_map/ppermute | solution.py:341
  36.9 6.6 %collective-permute-done.31 = bf16[32,2048]{1,0:T(8,128)(2,1)S(1)} collective-permute-done((bf16[32,2048]{1,0:T(8,128)(2,1)S(1)}, bf16[32,2048]{1,0:T(8,128)(2,1)S(1)}, u32[]{:S(2)}, u32[]{:S(2)}) %collective-permute-start.31) | collective-permute-done | bytes 131104 | tf_op jit(solution)/shard_map/ppermute | solution.py:341
  43.5 4.9 %collective-permute-start.8 = (bf16[32,2048]{1,0:T(8,128)(2,1)S(1)}, bf16[32,2048]{1,0:T(8,128)(2,1)S(1)}, u32[]{:S(2)}, u32[]{:S(2)}) collective-permute-start(bf16[32,2048]{1,0:T(8,128)(2,1)S(1)} %get-tuple-element.82), channel_id=1, source_target_pairs={{0,16},{2,18},{4,20},{6,22},{8,24},{10,26},{12,28},{14,30},{16,0},... | collective-permute-start | bytes 393224 | tf_op jit(solution)/shard_map/ppermute | solution.py:341
  48.4 8.6 %collective-permute-done.8 = bf16[32,2048]{1,0:T(8,128)(2,1)S(1)} collective-permute-done((bf16[32,2048]{1,0:T(8,128)(2,1)S(1)}, bf16[32,2048]{1,0:T(8,128)(2,1)S(1)}, u32[]{:S(2)}, u32[]{:S(2)}) %collective-permute-start.8) | collective-permute-done | bytes 131104 | tf_op jit(solution)/shard_map/ppermute | solution.py:341
  57.0 2.5 %collective-permute-start.23 = (bf16[32,2048]{1,0:T(8,128)(2,1)S(1)}, bf16[32,2048]{1,0:T(8,128)(2,1)S(1)}, u32[]{:S(2)}, u32[]{:S(2)}) collective-permute-start(bf16[32,2048]{1,0:T(8,128)(2,1)S(1)} %get-tuple-element.101), channel_id=1, source_target_pairs={{0,8},{2,10},{4,12},{6,14},{8,0},{10,2},{12,4},{14,6},{16,24},{18,... | collective-permute-start | bytes 393224 | tf_op jit(solution)/shard_map/ppermute | solution.py:341
  59.5 2.9 %collective-permute-done.23 = bf16[32,2048]{1,0:T(8,128)(2,1)S(1)} collective-permute-done((bf16[32,2048]{1,0:T(8,128)(2,1)S(1)}, bf16[32,2048]{1,0:T(8,128)(2,1)S(1)}, u32[]{:S(2)}, u32[]{:S(2)}) %collective-permute-start.23) | collective-permute-done | bytes 131104 | tf_op jit(solution)/shard_map/ppermute | solution.py:341
  62.5 4.3 %collective-permute-start.14 = (bf16[32,2048]{1,0:T(8,128)(2,1)S(1)}, bf16[32,2048]{1,0:T(8,128)(2,1)S(1)}, u32[]{:S(2)}, u32[]{:S(2)}) collective-permute-start(bf16[32,2048]{1,0:T(8,128)(2,1)S(1)} %get-tuple-element.91), channel_id=1, source_target_pairs={{0,4},{2,6},{4,0},{6,2},{8,12},{10,14},{12,8},{14,10},{16,20},{18,... | collective-permute-start | bytes 393224 | tf_op jit(solution)/shard_map/ppermute | solution.py:341
  67.2 4.8 %collective-permute-done.14 = bf16[32,2048]{1,0:T(8,128)(2,1)S(1)} collective-permute-done((bf16[32,2048]{1,0:T(8,128)(2,1)S(1)}, bf16[32,2048]{1,0:T(8,128)(2,1)S(1)}, u32[]{:S(2)}, u32[]{:S(2)}) %collective-permute-start.14) | collective-permute-done | bytes 131104 | tf_op jit(solution)/shard_map/ppermute | solution.py:341
  72.8 3.9 %collective-permute-start.10 = (bf16[32,2048]{1,0:T(8,128)(2,1)S(1)}, bf16[32,2048]{1,0:T(8,128)(2,1)S(1)}, u32[]{:S(2)}, u32[]{:S(2)}) collective-permute-start(bf16[32,2048]{1,0:T(8,128)(2,1)S(1)} %get-tuple-element.84), channel_id=1, source_target_pairs={{0,18},{2,16},{4,22},{6,20},{8,26},{10,24},{12,30},{14,28},{16,2},... | collective-permute-start | bytes 393224 | tf_op jit(solution)/shard_map/ppermute | solution.py:341
  76.7 7.1 %collective-permute-done.9 = bf16[32,2048]{1,0:T(8,128)(2,1)S(1)} collective-permute-done((bf16[32,2048]{1,0:T(8,128)(2,1)S(1)}, bf16[32,2048]{1,0:T(8,128)(2,1)S(1)}, u32[]{:S(2)}, u32[]{:S(2)}) %collective-permute-start.9) | collective-permute-done | bytes 131104 | tf_op jit(solution)/shard_map/ppermute | solution.py:341
  86.1 4.3 %collective-permute-start.24 = (bf16[32,2048]{1,0:T(8,128)(2,1)S(1)}, bf16[32,2048]{1,0:T(8,128)(2,1)S(1)}, u32[]{:S(2)}, u32[]{:S(2)}) collective-permute-start(bf16[32,2048]{1,0:T(8,128)(2,1)S(1)} %get-tuple-element.102), channel_id=1, source_target_pairs={{0,10},{2,8},{4,14},{6,12},{8,2},{10,0},{12,6},{14,4},{16,26},{18,... | collective-permute-start | bytes 393224 | tf_op jit(solution)/shard_map/ppermute | solution.py:341
  94.0 3.8 %collective-permute-done.25 = bf16[32,2048]{1,0:T(8,128)(2,1)S(1)} collective-permute-done((bf16[32,2048]{1,0:T(8,128)(2,1)S(1)}, bf16[32,2048]{1,0:T(8,128)(2,1)S(1)}, u32[]{:S(2)}, u32[]{:S(2)}) %collective-permute-start.25) | collective-permute-done | bytes 131104 | tf_op jit(solution)/shard_map/ppermute | solution.py:341
  99.4 5.1 %collective-permute-done.26 = bf16[32,2048]{1,0:T(8,128)(2,1)S(1)} collective-permute-done((bf16[32,2048]{1,0:T(8,128)(2,1)S(1)}, bf16[32,2048]{1,0:T(8,128)(2,1)S(1)}, u32[]{:S(2)}, u32[]{:S(2)}) %collective-permute-start.26) | collective-permute-done | bytes 131104 | tf_op jit(solution)/shard_map/ppermute | solution.py:341
  105.2 6.0 %shard_map.194 = (bf16[128,2048]{1,0:T(8,128)(2,1)S(1)}, bf16[128,2048]{1,0:T(8,128)(2,1)S(1)}) custom-call(bf16[128,2048]{1,0:T(8,128)(2,1)S(1)} %constant_dynamic-update-slice_fusion.8.refs_0_, bf16[128,2048]{1,0:T(8,128)(2,1)S(1)} %collective-permute-done.16.refs_1_, bf16[1,2048,1792]{2,1,0:T(8,128)(2,1)S(1)} %get-tuple-element.86.refs_2_, ...), custom_call_target="tpu_custom_call" | custom-call | flops 5637144576 | bytes 1048576 | tf_op jit(solution)/shard_map/pallas_call | solution.py:51
  111.2 6.0 %shard_map.195 = (bf16[128,2048]{1,0:T(8,128)(2,1)S(1)}, bf16[128,2048]{1,0:T(8,128)(2,1)S(1)}) custom-call(bf16[128,2048]{1,0:T(8,128)(2,1)S(1)} %constant_dynamic-update-slice_fusion.4.refs_0_, bf16[128,2048]{1,0:T(8,128)(2,1)S(1)} %collective-permute-done.12.refs_1_, bf16[1,2048,1792]{2,1,0:T(8,128)(2,1)S(1)} %get-tuple-element.86.refs_2_, ...), custom_call_target="tpu_custom_call" | custom-call | flops 5637144576 | bytes 1048576 | tf_op jit(solution)/shard_map/pallas_call | solution.py:51
  119.3 6.2 %shard_map.198 = (bf16[128,2048]{1,0:T(8,128)(2,1)S(1)}, bf16[128,2048]{1,0:T(8,128)(2,1)S(1)}) custom-call(bf16[128,2048]{1,0:T(8,128)(2,1)S(1)} %constant_dynamic-update-slice_fusion.12.refs_0_, bf16[128,2048]{1,0:T(8,128)(2,1)S(1)} %collective-permute-done.27.refs_1_, bf16[1,2048,1792]{2,1,0:T(8,128)(2,1)S(1)} %get-tuple-element.86.refs_2_, ...), custom_call_target="tpu_custom_call" | custom-call | flops 5637144576 | bytes 1048576 | tf_op jit(solution)/shard_map/pallas_call | solution.py:51
  125.7 6.0 %shard_map.201 = (bf16[128,2048]{1,0:T(8,128)(2,1)S(1)}, bf16[128,2048]{1,0:T(8,128)(2,1)S(1)}) custom-call(bf16[128,2048]{1,0:T(8,128)(2,1)S(1)} %constant_dynamic-update-slice_fusion.16.refs_0_, bf16[128,2048]{1,0:T(8,128)(2,1)S(1)} %collective-permute-done.35.refs_1_, bf16[1,2048,1792]{2,1,0:T(8,128)(2,1)S(1)} %get-tuple-element.86.refs_2_, ...), custom_call_target="tpu_custom_call" | custom-call | flops 5637144576 | bytes 1048576 | tf_op jit(solution)/shard_map/pallas_call | solution.py:51
  133.4 2.0 %collective-permute-start.29 = (bf16[32,2048]{1,0:T(8,128)(2,1)S(1)}, bf16[32,2048]{1,0:T(8,128)(2,1)S(1)}, u32[]{:S(2)}, u32[]{:S(2)}) collective-permute-start(bf16[32,2048]{1,0:T(8,128)(2,1)S(1)} %get-tuple-element.108), channel_id=1, source_target_pairs={{0,4},{2,6},{4,0},{6,2},{8,12},{10,14},{12,8},{14,10},{16,20},{18,... | collective-permute-start | bytes 393224 | tf_op jit(solution)/shard_map/ppermute | solution.py:341
  139.3 2.0 %collective-permute-start.20 = (bf16[32,2048]{1,0:T(8,128)(2,1)S(1)}, bf16[32,2048]{1,0:T(8,128)(2,1)S(1)}, u32[]{:S(2)}, u32[]{:S(2)}) collective-permute-start(bf16[32,2048]{1,0:T(8,128)(2,1)S(1)} %get-tuple-element.98), channel_id=1, source_target_pairs={{0,18},{2,16},{4,22},{6,20},{8,26},{10,24},{12,30},{14,28},{16,2},... | collective-permute-start | bytes 393224 | tf_op jit(solution)/shard_map/ppermute | solution.py:341
  141.4 2.5 %collective-permute-start.21 = (bf16[32,2048]{1,0:T(8,128)(2,1)S(1)}, bf16[32,2048]{1,0:T(8,128)(2,1)S(1)}, u32[]{:S(2)}, u32[]{:S(2)}) collective-permute-start(bf16[32,2048]{1,0:T(8,128)(2,1)S(1)} %get-tuple-element.99), channel_id=1, source_target_pairs={{0,26},{2,24},{4,30},{6,28},{8,18},{10,16},{12,22},{14,20},{16,10}... | collective-permute-start | bytes 393224 | tf_op jit(solution)/shard_map/ppermute | solution.py:341
  145.0 7.0 %collective-permute-done.18.refs_4_ = bf16[32,2048]{1,0:T(8,128)(2,1)S(1)} collective-permute-done((bf16[32,2048]{1,0:T(8,128)(2,1)S(1)}, bf16[32,2048]{1,0:T(8,128)(2,1)S(1)}, u32[]{:S(2)}, u32[]{:S(2)}) %collective-permute-start.18) | collective-permute-done | bytes 131104 | tf_op jit(solution)/shard_map/ppermute | solution.py:341
  152.0 3.5 %collective-permute-start.43 = (bf16[32,2048]{1,0:T(8,128)(2,1)S(1)}, bf16[32,2048]{1,0:T(8,128)(2,1)S(1)}, u32[]{:S(2)}, u32[]{:S(2)}) collective-permute-start(bf16[32,2048]{1,0:T(8,128)(2,1)S(1)} %get-tuple-element.122), channel_id=1, source_target_pairs={{0,10},{2,8},{4,14},{6,12},{8,2},{10,0},{12,6},{14,4},{16,26},{18,... | collective-permute-start | bytes 393224 | tf_op jit(solution)/shard_map/ppermute | solution.py:341
  157.6 4.3 %collective-permute-start.37 = (bf16[32,2048]{1,0:T(8,128)(2,1)S(1)}, bf16[32,2048]{1,0:T(8,128)(2,1)S(1)}, u32[]{:S(2)}, u32[]{:S(2)}) collective-permute-start(bf16[32,2048]{1,0:T(8,128)(2,1)S(1)} %get-tuple-element.116.refs_2_), channel_id=1, source_target_pairs={{0,20},{2,22},{4,16},{6,18},{8,28},{10,30},{12,24},{14,26},{16,4},... | collective-permute-start | bytes 393224 | tf_op jit(solution)/shard_map/ppermute | solution.py:341
  162.2 1.8 collective-permute-start.38
  164.1 6.3 %collective-permute-start.39 = (bf16[32,2048]{1,0:T(8,128)(2,1)S(1)}, bf16[32,2048]{1,0:T(8,128)(2,1)S(1)}, u32[]{:S(2)}, u32[]{:S(2)}) collective-permute-start(bf16[32,2048]{1,0:T(8,128)(2,1)S(1)} %get-tuple-element.118), channel_id=1, source_target_pairs={{0,22},{2,20},{4,18},{6,16},{8,30},{10,28},{12,26},{14,24},{16,6},... | collective-permute-start | bytes 393224 | tf_op jit(solution)/shard_map/ppermute | solution.py:341
  172.6 6.6 %collective-permute-done.38.refs_6_ = bf16[32,2048]{1,0:T(8,128)(2,1)S(1)} collective-permute-done((bf16[32,2048]{1,0:T(8,128)(2,1)S(1)}, bf16[32,2048]{1,0:T(8,128)(2,1)S(1)}, u32[]{:S(2)}, u32[]{:S(2)}) %collective-permute-start.38) | collective-permute-done | bytes 131104 | tf_op jit(solution)/shard_map/ppermute | solution.py:341
  180.3 4.5 %collective-permute-done.40.refs_8_ = bf16[32,2048]{1,0:T(8,128)(2,1)S(1)} collective-permute-done((bf16[32,2048]{1,0:T(8,128)(2,1)S(1)}, bf16[32,2048]{1,0:T(8,128)(2,1)S(1)}, u32[]{:S(2)}, u32[]{:S(2)}) %collective-permute-start.40) | collective-permute-done | bytes 131104 | tf_op jit(solution)/shard_map/ppermute | solution.py:341
  (103 shorter events, 35.3 us)
Async XLA Ops:
  0.0 19.2 %collective-permute-start.7 = (bf16[512,2048]{1,0:T(8,128)(2,1)}, bf16[512,2048]{1,0:T(8,128)(2,1)S(1)}, u32[]{:S(2)}, u32[]{:S(2)}) collective-permute-start(bf16[512,2048]{1,0:T(8,128)(2,1)} %refs_7_.3), channel_id=1, source_target_pairs={{0,1},{1,0},{2,3},{3,2},{4,5},{5,4},{6,7},{7,6},{8,9},{9,8},{10,11... | collective-permute-start | bytes 6291464 | tf_op jit(solution)/shard_map/ppermute | solution.py:336
  4.0 9.7 %collective-permute-start = (bf16[128,384]{1,0:T(8,128)(2,1)S(1)}, bf16[128,384]{1,0:T(8,128)(2,1)S(1)}, u32[]{:S(2)}, u32[]{:S(2)}) collective-permute-start(bf16[128,384]{1,0:T(8,128)(2,1)S(1)} %get-tuple-element.66), channel_id=1, source_target_pairs={{0,8},{2,10},{4,12},{6,14},{8,16},{10,18},{12,20},{14,22},{16,24},... | collective-permute-start | bytes 294920 | tf_op jit(solution)/shard_map/ppermute | solution.py:352
  5.6 8.0 %collective-permute-start.1 = (bf16[128,384]{1,0:T(8,128)(2,1)S(1)}, bf16[128,384]{1,0:T(8,128)(2,1)S(1)}, u32[]{:S(2)}, u32[]{:S(2)}) collective-permute-start(bf16[128,384]{1,0:T(8,128)(2,1)S(1)} %get-tuple-element.66), channel_id=1, source_target_pairs={{0,6},{2,8},{4,10},{6,12},{8,14},{10,16},{12,18},{14,20},{16,22},{... | collective-permute-start | bytes 294920 | tf_op jit(solution)/shard_map/ppermute | solution.py:352
  8.2 9.2 %collective-permute-start.3 = (bf16[128,384]{1,0:T(8,128)(2,1)S(1)}, bf16[128,384]{1,0:T(8,128)(2,1)S(1)}, u32[]{:S(2)}, u32[]{:S(2)}) collective-permute-start(bf16[128,384]{1,0:T(8,128)(2,1)S(1)} %get-tuple-element.66), channel_id=1, source_target_pairs={{0,2},{2,4},{4,6},{6,8},{8,10},{10,12},{12,14},{14,16},{16,18},{18... | collective-permute-start | bytes 294920 | tf_op jit(solution)/shard_map/ppermute | solution.py:352
  28.3 15.2 %collective-permute-start.31 = (bf16[32,2048]{1,0:T(8,128)(2,1)S(1)}, bf16[32,2048]{1,0:T(8,128)(2,1)S(1)}, u32[]{:S(2)}, u32[]{:S(2)}) collective-permute-start(bf16[32,2048]{1,0:T(8,128)(2,1)S(1)} %get-tuple-element.110), channel_id=1, source_target_pairs={{0,20},{2,22},{4,16},{6,18},{8,28},{10,30},{12,24},{14,26},{16,4},... | collective-permute-start | bytes 393224 | tf_op jit(solution)/shard_map/ppermute | solution.py:341
  28.4 88.8 %collective-permute-start.32 = (bf16[32,2048]{1,0:T(8,128)(2,1)S(1)}, bf16[32,2048]{1,0:T(8,128)(2,1)S(1)}, u32[]{:S(2)}, u32[]{:S(2)}) collective-permute-start(bf16[32,2048]{1,0:T(8,128)(2,1)S(1)} %get-tuple-element.111), channel_id=1, source_target_pairs={{0,28},{2,30},{4,24},{6,26},{8,20},{10,22},{12,16},{14,18},{16,12}... | collective-permute-start | bytes 393224 | tf_op jit(solution)/shard_map/ppermute | solution.py:341
  32.3 84.9 %collective-permute-start.33 = (bf16[32,2048]{1,0:T(8,128)(2,1)S(1)}, bf16[32,2048]{1,0:T(8,128)(2,1)S(1)}, u32[]{:S(2)}, u32[]{:S(2)}) collective-permute-start(bf16[32,2048]{1,0:T(8,128)(2,1)S(1)} %get-tuple-element.112), channel_id=1, source_target_pairs={{0,22},{2,20},{4,18},{6,16},{8,30},{10,28},{12,26},{14,24},{16,6},... | collective-permute-start | bytes 393224 | tf_op jit(solution)/shard_map/ppermute | solution.py:341
  32.6 84.6 %collective-permute-start.34 = (bf16[32,2048]{1,0:T(8,128)(2,1)S(1)}, bf16[32,2048]{1,0:T(8,128)(2,1)S(1)}, u32[]{:S(2)}, u32[]{:S(2)}) collective-permute-start(bf16[32,2048]{1,0:T(8,128)(2,1)S(1)} %get-tuple-element.113), channel_id=1, source_target_pairs={{0,30},{2,28},{4,26},{6,24},{8,22},{10,20},{12,18},{14,16},{16,14}... | collective-permute-start | bytes 393224 | tf_op jit(solution)/shard_map/ppermute | solution.py:341
  36.9 29.9 %collective-permute-start.13 = (bf16[32,2048]{1,0:T(8,128)(2,1)S(1)}, bf16[32,2048]{1,0:T(8,128)(2,1)S(1)}, u32[]{:S(2)}, u32[]{:S(2)}) collective-permute-start(bf16[32,2048]{1,0:T(8,128)(2,1)S(1)} %get-tuple-element.90), channel_id=1, source_target_pairs={{0,2},{2,0},{4,6},{6,4},{8,10},{10,8},{12,14},{14,12},{16,18},{18,... | collective-permute-start | bytes 393224 | tf_op jit(solution)/shard_map/ppermute | solution.py:341
  43.5 13.5 %collective-permute-start.8 = (bf16[32,2048]{1,0:T(8,128)(2,1)S(1)}, bf16[32,2048]{1,0:T(8,128)(2,1)S(1)}, u32[]{:S(2)}, u32[]{:S(2)}) collective-permute-start(bf16[32,2048]{1,0:T(8,128)(2,1)S(1)} %get-tuple-element.82), channel_id=1, source_target_pairs={{0,16},{2,18},{4,20},{6,22},{8,24},{10,26},{12,28},{14,30},{16,0},... | collective-permute-start | bytes 393224 | tf_op jit(solution)/shard_map/ppermute | solution.py:341
  62.5 9.5 %collective-permute-start.14 = (bf16[32,2048]{1,0:T(8,128)(2,1)S(1)}, bf16[32,2048]{1,0:T(8,128)(2,1)S(1)}, u32[]{:S(2)}, u32[]{:S(2)}) collective-permute-start(bf16[32,2048]{1,0:T(8,128)(2,1)S(1)} %get-tuple-element.91), channel_id=1, source_target_pairs={{0,4},{2,6},{4,0},{6,2},{8,12},{10,14},{12,8},{14,10},{16,20},{18,... | collective-permute-start | bytes 393224 | tf_op jit(solution)/shard_map/ppermute | solution.py:341
  72.0 11.8 %collective-permute-start.9 = (bf16[32,2048]{1,0:T(8,128)(2,1)S(1)}, bf16[32,2048]{1,0:T(8,128)(2,1)S(1)}, u32[]{:S(2)}, u32[]{:S(2)}) collective-permute-start(bf16[32,2048]{1,0:T(8,128)(2,1)S(1)} %get-tuple-element.83), channel_id=1, source_target_pairs={{0,24},{2,26},{4,28},{6,30},{8,16},{10,18},{12,20},{14,22},{16,8},... | collective-permute-start | bytes 393224 | tf_op jit(solution)/shard_map/ppermute | solution.py:341
  72.8 13.3 %collective-permute-start.10 = (bf16[32,2048]{1,0:T(8,128)(2,1)S(1)}, bf16[32,2048]{1,0:T(8,128)(2,1)S(1)}, u32[]{:S(2)}, u32[]{:S(2)}) collective-permute-start(bf16[32,2048]{1,0:T(8,128)(2,1)S(1)} %get-tuple-element.84), channel_id=1, source_target_pairs={{0,18},{2,16},{4,22},{6,20},{8,26},{10,24},{12,30},{14,28},{16,2},... | collective-permute-start | bytes 393224 | tf_op jit(solution)/shard_map/ppermute | solution.py:341
  83.8 8.1 %collective-permute-start.11 = (bf16[32,2048]{1,0:T(8,128)(2,1)S(1)}, bf16[32,2048]{1,0:T(8,128)(2,1)S(1)}, u32[]{:S(2)}, u32[]{:S(2)}) collective-permute-start(bf16[32,2048]{1,0:T(8,128)(2,1)S(1)} %get-tuple-element.85), channel_id=1, source_target_pairs={{0,26},{2,24},{4,30},{6,28},{8,18},{10,16},{12,22},{14,20},{16,10}... | collective-permute-start | bytes 393224 | tf_op jit(solution)/shard_map/ppermute | solution.py:341
  86.1 7.9 %collective-permute-start.24 = (bf16[32,2048]{1,0:T(8,128)(2,1)S(1)}, bf16[32,2048]{1,0:T(8,128)(2,1)S(1)}, u32[]{:S(2)}, u32[]{:S(2)}) collective-permute-start(bf16[32,2048]{1,0:T(8,128)(2,1)S(1)} %get-tuple-element.102), channel_id=1, source_target_pairs={{0,10},{2,8},{4,14},{6,12},{8,2},{10,0},{12,6},{14,4},{16,26},{18,... | collective-permute-start | bytes 393224 | tf_op jit(solution)/shard_map/ppermute | solution.py:341
  93.9 10.6 %collective-permute-start.16 = (bf16[128,2048]{1,0:T(8,128)(2,1)S(1)}, bf16[128,2048]{1,0:T(8,128)(2,1)S(1)}, u32[]{:S(2)}, u32[]{:S(2)}) collective-permute-start(bf16[128,2048]{1,0:T(8,128)(2,1)S(1)} %constant_dynamic-update-slice_fusion.8.refs_0_), channel_id=1, source_target_pairs={{0,1},{1,0},{2,3},{3,2},{4,5},{5,4},{6,7},{7,6},{8,9},{9,8},{10,11... | collective-permute-start | bytes 1572872 | tf_op jit(solution)/shard_map/ppermute | solution.py:336
  104.6 14.7 %collective-permute-start.27 = (bf16[128,2048]{1,0:T(8,128)(2,1)S(1)}, bf16[128,2048]{1,0:T(8,128)(2,1)S(1)}, u32[]{:S(2)}, u32[]{:S(2)}) collective-permute-start(bf16[128,2048]{1,0:T(8,128)(2,1)S(1)} %constant_dynamic-update-slice_fusion.12.refs_0_), channel_id=1, source_target_pairs={{0,1},{1,0},{2,3},{3,2},{4,5},{5,4},{6,7},{7,6},{8,9},{9,8},{10,11... | collective-permute-start | bytes 1572872 | tf_op jit(solution)/shard_map/ppermute | solution.py:336
  117.3 8.3 %collective-permute-start.35 = (bf16[128,2048]{1,0:T(8,128)(2,1)S(1)}, bf16[128,2048]{1,0:T(8,128)(2,1)S(1)}, u32[]{:S(2)}, u32[]{:S(2)}) collective-permute-start(bf16[128,2048]{1,0:T(8,128)(2,1)S(1)} %constant_dynamic-update-slice_fusion.16.refs_0_), channel_id=1, source_target_pairs={{0,1},{1,0},{2,3},{3,2},{4,5},{5,4},{6,7},{7,6},{8,9},{9,8},{10,11... | collective-permute-start | bytes 1572872 | tf_op jit(solution)/shard_map/ppermute | solution.py:336
  133.4 8.0 %collective-permute-start.29 = (bf16[32,2048]{1,0:T(8,128)(2,1)S(1)}, bf16[32,2048]{1,0:T(8,128)(2,1)S(1)}, u32[]{:S(2)}, u32[]{:S(2)}) collective-permute-start(bf16[32,2048]{1,0:T(8,128)(2,1)S(1)} %get-tuple-element.108), channel_id=1, source_target_pairs={{0,4},{2,6},{4,0},{6,2},{8,12},{10,14},{12,8},{14,10},{16,20},{18,... | collective-permute-start | bytes 393224 | tf_op jit(solution)/shard_map/ppermute | solution.py:341
  135.4 8.6 %collective-permute-start.30 = (bf16[32,2048]{1,0:T(8,128)(2,1)S(1)}, bf16[32,2048]{1,0:T(8,128)(2,1)S(1)}, u32[]{:S(2)}, u32[]{:S(2)}) collective-permute-start(bf16[32,2048]{1,0:T(8,128)(2,1)S(1)} %get-tuple-element.109), channel_id=1, source_target_pairs={{0,6},{2,4},{4,2},{6,0},{8,14},{10,12},{12,10},{14,8},{16,22},{18,... | collective-permute-start | bytes 393224 | tf_op jit(solution)/shard_map/ppermute | solution.py:341
  136.8 15.2 %collective-permute-start.18 = (bf16[32,2048]{1,0:T(8,128)(2,1)S(1)}, bf16[32,2048]{1,0:T(8,128)(2,1)S(1)}, u32[]{:S(2)}, u32[]{:S(2)}) collective-permute-start(bf16[32,2048]{1,0:T(8,128)(2,1)S(1)} %get-tuple-element.96.refs_1_), channel_id=1, source_target_pairs={{0,16},{2,18},{4,20},{6,22},{8,24},{10,26},{12,28},{14,30},{16,0},... | collective-permute-start | bytes 393224 | tf_op jit(solution)/shard_map/ppermute | solution.py:341
  137.5 19.3 %collective-permute-start.19 = (bf16[32,2048]{1,0:T(8,128)(2,1)S(1)}, bf16[32,2048]{1,0:T(8,128)(2,1)S(1)}, u32[]{:S(2)}, u32[]{:S(2)}) collective-permute-start(bf16[32,2048]{1,0:T(8,128)(2,1)S(1)} %get-tuple-element.97), channel_id=1, source_target_pairs={{0,24},{2,26},{4,28},{6,30},{8,16},{10,18},{12,20},{14,22},{16,8},... | collective-permute-start | bytes 393224 | tf_op jit(solution)/shard_map/ppermute | solution.py:341
  139.3 18.3 %collective-permute-start.20 = (bf16[32,2048]{1,0:T(8,128)(2,1)S(1)}, bf16[32,2048]{1,0:T(8,128)(2,1)S(1)}, u32[]{:S(2)}, u32[]{:S(2)}) collective-permute-start(bf16[32,2048]{1,0:T(8,128)(2,1)S(1)} %get-tuple-element.98), channel_id=1, source_target_pairs={{0,18},{2,16},{4,22},{6,20},{8,26},{10,24},{12,30},{14,28},{16,2},... | collective-permute-start | bytes 393224 | tf_op jit(solution)/shard_map/ppermute | solution.py:341
  141.4 20.5 %collective-permute-start.21 = (bf16[32,2048]{1,0:T(8,128)(2,1)S(1)}, bf16[32,2048]{1,0:T(8,128)(2,1)S(1)}, u32[]{:S(2)}, u32[]{:S(2)}) collective-permute-start(bf16[32,2048]{1,0:T(8,128)(2,1)S(1)} %get-tuple-element.99), channel_id=1, source_target_pairs={{0,26},{2,24},{4,30},{6,28},{8,18},{10,16},{12,22},{14,20},{16,10}... | collective-permute-start | bytes 393224 | tf_op jit(solution)/shard_map/ppermute | solution.py:341
  143.9 18.3 %collective-permute-start.42 = (bf16[32,2048]{1,0:T(8,128)(2,1)S(1)}, bf16[32,2048]{1,0:T(8,128)(2,1)S(1)}, u32[]{:S(2)}, u32[]{:S(2)}) collective-permute-start(bf16[32,2048]{1,0:T(8,128)(2,1)S(1)} %get-tuple-element.121), channel_id=1, source_target_pairs={{0,8},{2,10},{4,12},{6,14},{8,0},{10,2},{12,4},{14,6},{16,24},{18,... | collective-permute-start | bytes 393224 | tf_op jit(solution)/shard_map/ppermute | solution.py:341
  152.0 12.1 %collective-permute-start.43 = (bf16[32,2048]{1,0:T(8,128)(2,1)S(1)}, bf16[32,2048]{1,0:T(8,128)(2,1)S(1)}, u32[]{:S(2)}, u32[]{:S(2)}) collective-permute-start(bf16[32,2048]{1,0:T(8,128)(2,1)S(1)} %get-tuple-element.122), channel_id=1, source_target_pairs={{0,10},{2,8},{4,14},{6,12},{8,2},{10,0},{12,6},{14,4},{16,26},{18,... | collective-permute-start | bytes 393224 | tf_op jit(solution)/shard_map/ppermute | solution.py:341
  156.8 13.6 %collective-permute-start.44 = (bf16[32,2048]{1,0:T(8,128)(2,1)S(1)}, bf16[32,2048]{1,0:T(8,128)(2,1)S(1)}, u32[]{:S(2)}, u32[]{:S(2)}) collective-permute-start(bf16[32,2048]{1,0:T(8,128)(2,1)S(1)} %get-tuple-element.123), channel_id=1, source_target_pairs={{0,12},{2,14},{4,8},{6,10},{8,4},{10,6},{12,0},{14,2},{16,28},{18,... | collective-permute-start | bytes 393224 | tf_op jit(solution)/shard_map/ppermute | solution.py:341
  157.6 15.0 %collective-permute-start.37 = (bf16[32,2048]{1,0:T(8,128)(2,1)S(1)}, bf16[32,2048]{1,0:T(8,128)(2,1)S(1)}, u32[]{:S(2)}, u32[]{:S(2)}) collective-permute-start(bf16[32,2048]{1,0:T(8,128)(2,1)S(1)} %get-tuple-element.116.refs_2_), channel_id=1, source_target_pairs={{0,20},{2,22},{4,16},{6,18},{8,28},{10,30},{12,24},{14,26},{16,4},... | collective-permute-start | bytes 393224 | tf_op jit(solution)/shard_map/ppermute | solution.py:341
  161.9 10.7 %collective-permute-start.45 = (bf16[32,2048]{1,0:T(8,128)(2,1)S(1)}, bf16[32,2048]{1,0:T(8,128)(2,1)S(1)}, u32[]{:S(2)}, u32[]{:S(2)}) collective-permute-start(bf16[32,2048]{1,0:T(8,128)(2,1)S(1)} %get-tuple-element.124), channel_id=1, source_target_pairs={{0,14},{2,12},{4,10},{6,8},{8,6},{10,4},{12,2},{14,0},{16,30},{18,... | collective-permute-start | bytes 393224 | tf_op jit(solution)/shard_map/ppermute | solution.py:341
  162.2 17.0 %collective-permute-start.38 = (bf16[32,2048]{1,0:T(8,128)(2,1)S(1)}, bf16[32,2048]{1,0:T(8,128)(2,1)S(1)}, u32[]{:S(2)}, u32[]{:S(2)}) collective-permute-start(bf16[32,2048]{1,0:T(8,128)(2,1)S(1)} %get-tuple-element.117), channel_id=1, source_target_pairs={{0,28},{2,30},{4,24},{6,26},{8,20},{10,22},{12,16},{14,18},{16,12}... | collective-permute-start | bytes 393224 | tf_op jit(solution)/shard_map/ppermute | solution.py:341
  164.1 16.3 %collective-permute-start.39 = (bf16[32,2048]{1,0:T(8,128)(2,1)S(1)}, bf16[32,2048]{1,0:T(8,128)(2,1)S(1)}, u32[]{:S(2)}, u32[]{:S(2)}) collective-permute-start(bf16[32,2048]{1,0:T(8,128)(2,1)S(1)} %get-tuple-element.118), channel_id=1, source_target_pairs={{0,22},{2,20},{4,18},{6,16},{8,30},{10,28},{12,26},{14,24},{16,6},... | collective-permute-start | bytes 393224 | tf_op jit(solution)/shard_map/ppermute | solution.py:341
  170.4 14.5 %collective-permute-start.40 = (bf16[32,2048]{1,0:T(8,128)(2,1)S(1)}, bf16[32,2048]{1,0:T(8,128)(2,1)S(1)}, u32[]{:S(2)}, u32[]{:S(2)}) collective-permute-start(bf16[32,2048]{1,0:T(8,128)(2,1)S(1)} %get-tuple-element.119), channel_id=1, source_target_pairs={{0,30},{2,28},{4,26},{6,24},{8,22},{10,20},{12,18},{14,16},{16,14}... | collective-permute-start | bytes 393224 | tf_op jit(solution)/shard_map/ppermute | solution.py:341
  (16 other events, 181.8 us)
